TPU v7x, 128 devices: a whole 4x4x4 slice. The times are simulated.
128 devices in a mesh: sp: 32 (over z, y, core), tp: 4 (over x).
Axes of the slice: x: 4, y: 4, z: 4, core: 2. Of those that a mesh axis runs over, the one named last changes fastest.
Arguments:
- queries: bfloat16 [16384, 2048], P('sp', 'tp'), may hold values from -6 to 6
- keys: bfloat16 [16384, 2048], P('sp', 'tp'), may hold values from -6 to 6
- values: bfloat16 [16384, 2048], P('sp', 'tp'), may hold values from -6 to 6
- output_gate_logits: bfloat16 [16384, 2048], P('sp', 'tp'), may hold values from -6 to 6
- decay_gate_logits: float32 [2, 16384, 16], P(None, 'sp', 'tp'), may hold values from -6 to 6
- write_strength_logits: float32 [2, 16384, 16], P(None, 'sp', 'tp'), may hold values from -7 to -4
- extra_log_decay: float32 [2, 16384, 16], P(None, 'sp', 'tp'), may hold values from -2.1 to 0
- head_decay_rate: float32 [2, 16], P(None, 'tp'), may hold values from 0 to 0.04
- head_norm_gain: bfloat16 [128], replicated, may hold values from 0.099609375 to 1.8984375
- output_weight: bfloat16 [2048, 4096], P('tp'), may hold values from -0.125 to 0.125
- residual: bfloat16 [16384, 4096], P(('sp', 'tp')), may hold values from -6 to 6
- expert_norm_gain: bfloat16 [4096], replicated, may hold values from 0.099609375 to 1.8984375
- selected_experts: int32 [16384, 2], P(('sp', 'tp')), may hold values from 0 to 31, all different within a row; in each aligned block of 128 rows (0 to 127, 128 to 255, ...) at most 12 rows name the same one
- router_chosen_scores: float32 [16384, 2], P(('sp', 'tp')), may hold values from -6 to 6
- gate_up_weight: bfloat16 [32, 4096, 1536], P('sp', None, 'tp'), may hold values from -0.75 to 0.75
- linear_up_weight: bfloat16 [32, 4096, 1536], P('sp', None, 'tp'), may hold values from -0.375 to 0.375
- down_weight: bfloat16 [32, 1536, 4096], P('sp', 'tp'), may hold values from -0.009765625 to 0.009765625
Outputs:
- block_out: bfloat16 [16384, 4096], P(('sp', 'tp'))
Inputs may be any that keep to these rules, and one draw needn't show every extreme that they name: `selected_experts`: each row names 2 different experts. In each aligned block of rows that one device holds, no expert is named by more than 12 rows, and in every draw some expert is named by exactly 12 rows of some block.
All inputs are finite; a program needn't handle non-finite values.
Results may differ from a plain program's by a relative error of at most 0.02.
Values may be sent and summed in bfloat16 or wider, within the bound.
A program may use at most 128 MiB of HBM per device.

v0:
```python
import jax
import jax.numpy as jnp
from jax import lax
from jax.sharding import Mesh
from jax.sharding import PartitionSpec as P

HEAD_DIM = 128
TOPK = 2
BLOCK = 128
SP = ("sp_0", "sp_1", "sp_2")
SP_TP = ("sp_0", "sp_1", "sp_2", "tp")


def filled_with(shard, identity):
    return jax.tree.map(
        lambda part, zero: jnp.zeros_like(part) + jnp.asarray(zero, part.dtype), shard, identity
    )


def entering(shard, axes, combine, identity):
    before = start = filled_with(shard, identity)
    total = shard
    for axis in reversed(axes):
        count, here = (lax.axis_size(axis), lax.axis_index(axis))
        pieces = jax.tree.map(
            lambda part, kind: lax.all_gather(part.astype(kind), axis),
            total,
            (jnp.bfloat16, jnp.bfloat16),
        )
        inside, total = (start, start)
        for k in range(count):
            passed = k < here
            total = combine(
                total, jax.tree.map(lambda part, own: part[k].astype(own.dtype), pieces, shard)
            )
            inside = jax.tree.map(lambda new, old: jnp.where(passed, new, old), total, inside)
        before = combine(inside, before)
    return before


def entering_2(shard, axis, combine, identity):
    count, here = (lax.axis_size(axis), lax.axis_index(axis))
    everything = jax.tree.map(
        lambda part, kind: lax.all_gather(part.astype(kind), axis),
        shard,
        (jnp.bfloat16, jnp.bfloat16),
    )
    start = jax.tree.map(
        lambda part, zero: jnp.broadcast_to(jnp.asarray(zero, part.dtype), part.shape),
        shard,
        identity,
    )

    def turn(k, before):
        at = count - 1 - k
        reached = at > here
        new = combine(
            before, jax.tree.map(lambda part, own: part[at].astype(own.dtype), everything, shard)
        )
        return jax.tree.map(lambda a, b: jnp.where(reached, a, b), new, before)

    return lax.fori_loop(0, count, turn, start)


def in_blocks(shard, dim, count):
    shape = shard.shape
    parts = shard.reshape(*shape[:dim], count, shape[dim] // count, *shape[dim + 1 :])
    return jnp.moveaxis(parts, dim, 0)


def summed_on_arrival(shard, axis, dim):
    parts = in_blocks(shard, dim, lax.axis_size(axis))
    arrived = lax.all_to_all(parts, axis, split_axis=0, concat_axis=0, tiled=True)
    return arrived.astype(jnp.float32).sum(axis=0)


def unit_rows(tensor):
    return tensor * lax.rsqrt(jnp.sum(tensor * tensor, axis=-1, keepdims=True) + 1e-06)


def prepare(query_blk, key_blk, value_blk, log_blk, beta_blk):
    cumulative = jnp.cumsum(log_blk, axis=-1)
    position = jnp.arange(log_blk.shape[-1])
    inclusive = position[:, None] >= position[None, :]
    strict = position[:, None] > position[None, :]
    log_gap = cumulative[..., :, None] - cumulative[..., None, :]
    decay_mat = jnp.where(inclusive, jnp.exp(jnp.where(inclusive, log_gap, 0.0)), 0.0)
    key_beta = key_blk * beta_blk[..., None]
    lower_part = jnp.where(
        strict, jnp.einsum("hnid,hnjd->hnij", key_beta, key_blk) * decay_mat, 0.0
    )
    lower_mat = lower_part + jnp.eye(log_blk.shape[-1], dtype=jnp.float32)
    corrected = lax.linalg.triangular_solve(
        lower_mat, value_blk * beta_blk[..., None], left_side=True, lower=True, unit_diagonal=True
    )
    weighted = lax.linalg.triangular_solve(
        lower_mat,
        key_beta * jnp.exp(cumulative)[..., None],
        left_side=True,
        lower=True,
        unit_diagonal=True,
    )
    block_decay = cumulative[..., -1]
    key_end = key_blk * jnp.exp(block_decay[..., None] - cumulative)[..., None]
    query_decay = query_blk * jnp.exp(cumulative)[..., None]
    query_key = jnp.where(
        inclusive, jnp.einsum("hnid,hnjd->hnij", query_blk, key_blk) * decay_mat, 0.0
    )
    return (corrected, weighted, key_end, block_decay, query_decay, query_key)


def block_sweep(parts, state, transfer, track_map, emit_out):
    by_block = tuple((jnp.moveaxis(tensor, 1, 0) for tensor in parts))

    def block_step(carried, block_parts):
        state_now, transfer_now = carried
        corrected, weighted, key_end, block_decay, query_decay, query_key = block_parts
        carry_scale = jnp.exp(block_decay)[:, None, None]
        fresh_values = corrected - jnp.einsum("hid,hde->hie", weighted, state_now)
        state_next = carry_scale * state_now + jnp.einsum("hid,hie->hde", key_end, fresh_values)
        emitted = ()
        if emit_out:
            emitted = emitted + (
                jnp.einsum("hid,hde->hie", query_decay, state_now)
                + jnp.einsum("hij,hje->hie", query_key, fresh_values),
            )
        transfer_next = transfer_now
        if track_map:
            moved_map = jnp.einsum("hid,hde->hie", weighted, transfer_now)
            transfer_next = carry_scale * transfer_now - jnp.einsum(
                "hid,hie->hde", key_end, moved_map
            )
        return ((state_next, transfer_next), emitted)

    return lax.scan(block_step, (state, transfer), by_block)


def combine(earlier_pair, later_pair):
    map_part = jnp.einsum("hij,hjk->hik", later_pair[0], earlier_pair[0])
    state_part = jnp.einsum("hij,hjk->hik", later_pair[0], earlier_pair[1]) + later_pair[1]
    return (map_part, state_part)


def per_device(
    queries,
    keys,
    values,
    output_gate_logits,
    decay_gate_logits,
    write_strength_logits,
    extra_log_decay,
    head_decay_rate,
    head_norm_gain,
    output_weight,
    residual,
    expert_norm_gain,
    selected_experts,
    router_chosen_scores,
    gate_up_weight,
    linear_up_weight,
    down_weight,
):
    tok_rows, width_dev = queries.shape
    head_count = width_dev // HEAD_DIM
    nblocks = tok_rows // BLOCK

    def split_heads(tensor):
        return tensor.astype(jnp.float32).reshape(tok_rows, head_count, HEAD_DIM).transpose(1, 0, 2)

    def reverse_tokens(tensor):
        return jnp.flip(tensor, axis=1)

    def to_blocks(tensor):
        return tensor.reshape((head_count, nblocks, BLOCK) + tensor.shape[2:])

    def to_tokens(stacked):
        return jnp.moveaxis(stacked, 0, 1).reshape(head_count, tok_rows, -1)

    query_heads = unit_rows(split_heads(queries)) * HEAD_DIM ** (-0.5)
    key_heads = unit_rows(split_heads(keys))
    value_heads = split_heads(values)
    decay_logarithm = (
        -head_decay_rate[:, None, :] * jax.nn.softplus(decay_gate_logits) + extra_log_decay
    ).transpose(0, 2, 1)
    beta_gate = jax.nn.sigmoid(write_strength_logits).transpose(0, 2, 1)
    forward_parts = prepare(
        to_blocks(query_heads),
        to_blocks(key_heads),
        to_blocks(value_heads),
        to_blocks(decay_logarithm[0]),
        to_blocks(beta_gate[0]),
    )
    backward_parts = prepare(
        to_blocks(reverse_tokens(query_heads)),
        to_blocks(reverse_tokens(key_heads)),
        to_blocks(reverse_tokens(value_heads)),
        to_blocks(reverse_tokens(decay_logarithm[1])),
        to_blocks(reverse_tokens(beta_gate[1])),
    )
    unit_maps = jnp.broadcast_to(
        jnp.eye(HEAD_DIM, dtype=jnp.float32), (head_count, HEAD_DIM, HEAD_DIM)
    )
    zero_state = jnp.zeros((head_count, HEAD_DIM, HEAD_DIM), jnp.float32)
    forward_final, forward_local = block_sweep(forward_parts, zero_state, unit_maps, True, False)
    backward_final, backward_local = block_sweep(backward_parts, zero_state, unit_maps, True, False)
    forward_in = entering(
        (forward_final[1], forward_final[0]), SP, combine, (unit_maps, zero_state)
    )
    backward_in = entering_2(
        (backward_final[1], backward_final[0]), SP, combine, (unit_maps, zero_state)
    )
    forward_blocks = block_sweep(forward_parts, forward_in[1], unit_maps, False, True)[1][0]
    backward_blocks = block_sweep(backward_parts, backward_in[1], unit_maps, False, True)[1][0]
    summed_heads = (
        to_tokens(forward_blocks) + reverse_tokens(to_tokens(backward_blocks))
    ).transpose(1, 0, 2)
    scaled_heads = (
        summed_heads
        * lax.rsqrt(jnp.mean(summed_heads * summed_heads, axis=-1, keepdims=True) + 1e-06)
        * head_norm_gain.astype(jnp.float32)
    )
    gate_heads = output_gate_logits.astype(jnp.float32).reshape(tok_rows, head_count, HEAD_DIM)
    head_mix = (
        (scaled_heads * jax.nn.silu(gate_heads)).reshape(tok_rows, width_dev).astype(jnp.bfloat16)
    )
    local_rows = residual.shape[0]
    mix_sum = summed_on_arrival(
        jnp.dot(head_mix, output_weight, preferred_element_type=jnp.float32).astype(jnp.bfloat16),
        "tp",
        0,
    )
    stream = (residual.astype(jnp.float32) + mix_sum).astype(jnp.bfloat16)
    stream_wide = stream.astype(jnp.float32)
    normed = (
        stream_wide
        * lax.rsqrt(jnp.mean(stream_wide * stream_wide, axis=-1, keepdims=True) + 1e-06)
        * expert_norm_gain.astype(jnp.float32)
    ).astype(jnp.bfloat16)
    route_exp = jnp.exp(router_chosen_scores)
    route_weight = route_exp / jnp.sum(route_exp, axis=-1, keepdims=True)
    sp_count = lax.axis_size(SP)
    tp_count = lax.axis_size("tp")
    exp_dev = gate_up_weight.shape[0]
    experts = exp_dev * sp_count
    capacity = 3 * TOPK * tok_rows // (2 * tp_count * experts)
    model_width = normed.shape[1]
    flat_experts = selected_experts.reshape(-1)
    member = (flat_experts[:, None] == jnp.arange(experts, dtype=jnp.int32)[None, :]).astype(
        jnp.int32
    )
    slot_rank = jnp.sum(jnp.cumsum(member, axis=0) * member, axis=1) - 1
    slot_index = flat_experts * capacity + slot_rank
    slot_hot = (
        slot_index[:, None] == jnp.arange(experts * capacity, dtype=jnp.int32)[None, :]
    ).astype(jnp.bfloat16)
    token_hot = jnp.sum(slot_hot.reshape(local_rows, TOPK, experts * capacity), axis=1)
    outgoing = jnp.einsum(
        "rs,rd->sd", token_hot, normed, preferred_element_type=jnp.float32
    ).astype(jnp.bfloat16)
    grouped = outgoing.reshape(sp_count, exp_dev, capacity, model_width)
    copies = jnp.broadcast_to(
        grouped[:, None], (sp_count, tp_count, exp_dev, capacity, model_width)
    )
    copies = copies.reshape(sp_count * tp_count, exp_dev, capacity, model_width)
    arrived = lax.all_to_all(copies, SP_TP, split_axis=0, concat_axis=0, tiled=True)
    gate_pre = jnp.einsum(
        "secd,edf->secf", arrived, gate_up_weight, preferred_element_type=jnp.float32
    )
    linear_pre = jnp.einsum(
        "secd,edf->secf", arrived, linear_up_weight, preferred_element_type=jnp.float32
    )
    clipped = jnp.minimum(gate_pre, 7.0)
    hidden_act = (
        clipped * jax.nn.sigmoid(1.702 * clipped) * (jnp.clip(linear_pre, -7.0, 7.0) + 1.0)
    ).astype(jnp.bfloat16)
    partial_value = jnp.einsum(
        "secf,efd->secd", hidden_act, down_weight, preferred_element_type=jnp.float32
    )
    summed = lax.psum_scatter(
        partial_value.reshape(sp_count, tp_count, exp_dev, capacity, model_width).astype(
            jnp.bfloat16
        ),
        "tp",
        scatter_dimension=1,
        tiled=True,
    )
    returned = lax.all_to_all(summed, SP, split_axis=0, concat_axis=0, tiled=True)
    returned = returned.reshape(experts * capacity, model_width)
    picked = jnp.dot(slot_hot, returned, preferred_element_type=jnp.float32).reshape(
        local_rows, TOPK, model_width
    )
    combined = jnp.sum(picked * route_weight[:, :, None], axis=1)
    return (stream_wide + combined).astype(jnp.bfloat16)


def solution(mesh):
    torus = Mesh(mesh.devices.reshape(4, 4, 2, mesh.shape["tp"]), ("sp_0", "sp_1", "sp_2", "tp"))
    placed = (
        P(SP, "tp"),
        P(SP, "tp"),
        P(SP, "tp"),
        P(SP, "tp"),
        P(None, SP, "tp"),
        P(None, SP, "tp"),
        P(None, SP, "tp"),
        P(None, "tp"),
        P(),
        P("tp", None),
        P(SP_TP, None),
        P(),
        P(SP_TP, None),
        P(SP_TP, None),
        P(SP, None, "tp"),
        P(SP, None, "tp"),
        P(SP, "tp", None),
    )
    return jax.shard_map(
        per_device, mesh=torus, in_specs=placed, out_specs=P(SP_TP, None), check_vma=False
    )
```

profile of v0, /device:TPU:0, one launch (start us, length us, event | category | flops | bytes accessed | tf_op | source)
XLA Modules:
  0.0 1208.2 jit_solution(11840151258301023051)
XLA Ops:
  6.7 2.2 copy.334
  10.0 2.2 fusion.191
  14.5 2.1 convert_bitcast_fusion.1
  19.9 2.6 broadcast_multiply_fusion.1
  22.6 9.3 rev.21
  31.9 2.5 copy.358
  36.6 3.3 fusion.156
  39.9 158.6 %custom-call.11 = f32[4,4,1,128,128]{3,4,2,1,0:T(8,128)} custom-call(f32[4,4,1,128,128]{4,3,2,1,0:T(8,128)} %fusion.156), custom_call_target="InvertDiagBlocksLowerTriangular" | custom-call | tf_op jit(solution)/shard_map/triangular_solve/custom-call.1 | solution.py:93
  198.6 3.9 convolution_bitcast_fusion.1
  203.4 9.4 rev.23
  212.8 2.5 copy.360
  215.4 3.7 convolution_bitcast_fusion.2
  220.2 9.3 reverse.3
  229.5 2.4 broadcast_multiply_fusion
  231.9 2.5 copy.367
  234.4 2.7 multiply_bitcast_fusion
  240.0 24.1 %while.69 = (s32[]{:T(128)}, f32[4,128,128]{2,1,0:T(8,128)}, f32[4,128,128]{2,1,0:T(8,128)}, f32[4,4]{1,0:T(4,128)S(1)}, bf16[4,4,128,128]{2,3,1,0:T(8,128)(2,1)...) while((s32[]{:T(128)}, f32[4,128,128]{2,1,0:T(8,128)}, ...), condition=%wide.region_9.11_spmd.clone, body=%wide.region_8.10_spmd.clone.sunk | while | flops 67633152 | bytes 3412618 | solution.py:135
  241.0 2.1 convolution_add_fusion.25
  267.7 2.6 copy.335
  270.3 2.6 copy.338
  274.3 3.4 fusion.171
  277.7 158.6 %custom-call.9 = f32[4,4,1,128,128]{3,4,2,1,0:T(8,128)} custom-call(f32[4,4,1,128,128]{4,3,2,1,0:T(8,128)} %fusion.171), custom_call_target="InvertDiagBlocksLowerTriangular" | custom-call | tf_op jit(solution)/shard_map/triangular_solve/custom-call.1 | solution.py:93
  436.4 4.1 convolution_bitcast_fusion.4
  441.3 2.1 convolution_bitcast_fusion.5
  448.6 31.2 %while.68 = (s32[]{:T(128)}, f32[4,128,128]{2,1,0:T(8,128)}, f32[4,128,128]{2,1,0:T(8,128)}, f32[4,4]{1,0:T(4,128)S(1)}, bf16[4,4,128,128]{2,3,1,0:T(8,128)(2,1)...) while((s32[]{:T(128)}, f32[4,128,128]{2,1,0:T(8,128)}, ...), condition=%wide.region_3.5_spmd.clone, body=%wide.region_2.0_spmd.clone.sunk | while | flops 67633152 | bytes 3411626 | solution.py:135
  450.2 2.2 convolution_add_fusion.24
  454.1 2.2 convolution_subtract_fusion.12
  458.0 2.3 convolution_add_fusion.24
  461.9 2.2 convolution_subtract_fusion.12
  465.8 2.3 convolution_add_fusion.24
  469.8 2.2 convolution_subtract_fusion.12
  473.7 2.3 convolution_add_fusion.24
  477.6 2.2 convolution_subtract_fusion.12
  487.8 13.4 %all-gather.4 = bf16[16,128,128]{2,1,0:T(8,128)(2,1)S(1)} all-gather(bf16[4,128,128]{2,1,0:T(8,128)(2,1)S(1)} %convolution_add_fusion.13), channel_id=6, replica_groups=mesh['sp_0'=4,'sp_1'=4,'sp_2'=2,'tp'=4] {'sp_1'}, dimensions={0}, use_global_device_ids=true | all-gather | bytes 655360 | tf_op jit(solution)/shard_map/all_gather | solution.py:26
  501.2 13.1 %all-gather.1 = bf16[16,128,128]{2,1,0:T(8,128)(2,1)S(1)} all-gather(bf16[4,128,128]{2,1,0:T(8,128)(2,1)S(1)} %fusion.287), channel_id=3, replica_groups=mesh['sp_0'=4,'sp_1'=4,'sp_2'=2,'tp'=4] {'sp_1'}, dimensions={0}, use_global_device_ids=true | all-gather | bytes 655360 | tf_op jit(solution)/shard_map/all_gather | solution.py:26
  516.6 2.5 copy.347
  521.2 2.2 copy.380
  523.5 14.3 %all-gather.5 = bf16[16,128,128]{2,1,0:T(8,128)(2,1)S(1)} all-gather(bf16[4,128,128]{2,1,0:T(8,128)(2,1)} %convolution_add_fusion.10), channel_id=7, replica_groups=mesh['sp_0'=4,'sp_1'=4,'sp_2'=2,'tp'=4] {'sp_0'}, dimensions={0}, use_global_device_ids=true | all-gather | bytes 655360 | tf_op jit(solution)/shard_map/all_gather | solution.py:26
  541.3 13.2 %all-gather.2 = bf16[16,128,128]{2,1,0:T(8,128)(2,1)S(1)} all-gather(bf16[4,128,128]{2,1,0:T(8,128)(2,1)S(1)} %fusion.290), channel_id=4, replica_groups=mesh['sp_0'=4,'sp_1'=4,'sp_2'=2,'tp'=4] {'sp_0'}, dimensions={0}, use_global_device_ids=true | all-gather | bytes 655360 | tf_op jit(solution)/shard_map/all_gather | solution.py:26
  561.1 2.4 multiply_bitcast_fusion.2
  563.5 2.9 fusion.143
  568.9 24.9 %while.66 = (s32[]{:T(128)}, f32[4,128,128]{2,1,0:T(8,128)}, f32[4,4,128,128]{3,2,0,1:T(8,128)}, f32[4,4]{1,0:T(4,128)S(1)}, bf16[4,4,128,128]{2,3,1,0:T(8,128)(...) while((s32[]{:T(128)}, f32[4,128,128]{2,1,0:T(8,128)}, ...), condition=%wide.region_6.8_spmd, body=%wide.region_5.7_spmd.sunk | while | flops 67436544 | bytes 3017881 | solution.py:135
  593.8 38.9 %while.70 = (s32[]{:T(128)}, f32[4,128,128]{2,1,0:T(8,128)S(1)}, s32[]{:T(128)}, bf16[32,4,128,128]{3,2,1,0:T(8,128)(2,1)}, bf16[32,4,128,128]{3,2,1,0:T(8,128)(...) while((s32[]{:T(128)}, f32[4,128,128]{2,1,0:T(8,128)S(1)}, s32[]{:T(128)}, ...), condition=%wide.region_11.13_spmd.clone, body=%wide.region_10.12_spmd.clone.sunk | while | flops 17104904 | bytes 1575581 | solution.py:62
  633.7 21.0 %while.67 = (s32[]{:T(128)}, f32[4,128,128]{2,1,0:T(8,128)S(1)}, f32[4,4,128,128]{3,2,0,1:T(8,128)}, f32[4,4]{1,0:T(4,128)S(1)}, bf16[4,4,128,128]{2,3,1,0:T(8,1...) while((s32[]{:T(128)}, f32[4,128,128]{2,1,0:T(8,128)S(1)}, ...), condition=%wide.region_13.15_spmd, body=%wide.region_12.14_spmd.sunk | while | flops 67436544 | bytes 3017881 | solution.py:135
  654.8 8.9 rev.25
  669.4 6.7 convolution_convert_fusion
  676.1 5.0 all-to-all-start
  682.8 36.9 %all-to-all-done = bf16[4,128,4096]{2,1,0:T(8,128)(2,1)} async-done(((bf16[4,128,4096]{2,1,0:T(8,128)(2,1)}), bf16[4,128,4096]{2,1,0:T(8,128)(2,1)}, u32[]{:S(2)}, u32[]{:S(2)}) %all-to-all-start) | async-done | bytes 4194336 | tf_op jit(solution)/shard_map/all_to_all | solution.py:73
  719.7 3.3 convert_reduce_fusion
  724.4 2.8 convolution_convert_fusion.1
  727.2 5.5 broadcast_in_dim.121
  732.6 4.2 broadcast_in_dim.122
  736.9 195.6 %all_to_all.15 = bf16[128,1,12,4096]{3,2,1,0:T(8,128)(2,1)S(1)} all-to-all(bf16[128,1,12,4096]{3,2,1,0:T(8,128)(2,1)S(1)} %bitcast.435), channel_id=1, replica_groups=mesh['sp_0'=4,'sp_1'=4,'sp_2'=2,'tp'=4] {'sp_0','sp_1','sp_2','tp'}, dimensions={0} | all-to-all | bytes 25165824 | tf_op jit(solution)/shard_map/all_to_all | solution.py:265
  932.5 5.7 copy-done.2
  938.2 16.1 %fusion.104 = f32[128,12,384]{2,0,1:T(8,128)} fusion(bf16[128,1,12,4096]{3,2,1,0:T(8,128)(2,1)S(1)} %all_to_all.15, bf16[1,4096,384]{2,1,0:T(8,128)(2,1)S(1)} %copy-done.40), kind=kOutput, calls=%fused_computation.99 | convolution fusion | flops 4831838208 | bytes 18087936 | tf_op jit(solution)/shard_map/secd,edf->secf/dot_general | solution.py:266
  954.3 25.9 %convert_bitcast_fusion = bf16[128,1,12,4096]{3,0,2,1:T(8,128)(2,1)} fusion(bf16[1,384,4096]{2,1,0:T(8,128)(2,1)S(1)} %copy-done, bf16[1,4096,384]{2,1,0:T(8,128)(2,1)} %param.44, bf16[128,1,12,4096]{3,2,1,0:T(8,128)(2,1)} %copy-done.2, f32[128,12,384]{2,0,1:T(8,128)} %fusion.104), kind=kOutput, calls=%fused_computation.101 | convolution fusion | flops 9675866112 | bytes 33816576 | tf_op jit(solution)/shard_map/secf,efd->secd/dot_general | solution.py:276
  980.2 19.0 %convert_element_type.261 = bf16[32,4,1,12,4096]{4,1,0,3,2:T(4,128)(2,1)} reshape(bf16[128,1,12,4096]{3,0,2,1:T(8,128)(2,1)} %convert_bitcast_fusion) | data formatting | bytes 25165824 | tf_op jit(solution)/shard_map/convert_element_type | solution.py:280
  999.1 14.7 %copy.387 = bf16[32,4,1,12,4096]{4,0,3,2,1:T(8,128)(2,1)} copy(bf16[32,4,1,12,4096]{4,1,0,3,2:T(4,128)(2,1)} %convert_element_type.261) | data formatting | bytes 25165824 | tf_op jit(solution)/shard_map/convert_element_type | solution.py:280
  1013.9 109.8 %reduce-scatter.2.cloned.1.call-done = bf16[32,1,1,12,4096]{4,0,3,2,1:T(8,128)(2,1)} async-done(((bf16[32,4,1,12,4096]{4,0,3,2,1:T(8,128)(2,1)}), bf16[32,1,1,12,4096]{4,0,3,2,1:T(8,128)(2,1)}) %reduce-scatter.2.cloned.1.call-update) | async-done | bytes 3145744 | tf_op jit(solution)/shard_map/reduce_scatter | solution.py:279
  1123.7 5.7 copy.388
  1129.4 7.5 all-to-all-start.2
  1136.9 53.9 %all-to-all-done.2 = bf16[32,1,1,12,4096]{4,3,2,1,0:T(8,128)(2,1)} async-done(((bf16[32,1,1,12,4096]{4,3,2,1,0:T(8,128)(2,1)}), bf16[32,1,1,12,4096]{4,3,2,1,0:T(8,128)(2,1)}, u32[]{:S(2)}, u32[]{:S(2)}) %all-to-all-start.2) | async-done | bytes 3145760 | tf_op jit(solution)/shard_map/all_to_all | solution.py:287
  1190.9 5.6 reshape.393
  1196.4 3.6 fusion.120
  (325 shorter events, 179.2 us)
Async XLA Ops:
  6.5 947.8 %copy-start = (bf16[1,384,4096]{2,1,0:T(8,128)(2,1)S(1)}, bf16[1,384,4096]{2,1,0:T(8,128)(2,1)}, u32[]{:S(2)}) copy-start(bf16[1,384,4096]{2,1,0:T(8,128)(2,1)} %param.45) | copy-start | bytes 9437188
  6.5 5.7 copy-start.38
  6.5 5.7 copy-start.33
  6.5 5.7 copy-start.32
  6.5 5.9 copy-start.34
  6.5 587.2 %all-gather.11.cloned.1.call-start = ((), (), s32[]{:S(2)}) async-start(), calls=%async_computation.5 | async-start | bytes 4325376 | tf_op jit(solution)/shard_map/all_gather | solution.py:44
  6.6 29.9 %copy-start.31 = (f32[128,128]{1,0:T(8,128)}, f32[128,128]{1,0:T(8,128)S(1)}, u32[]{:S(2)}) copy-start(f32[128,128]{1,0:T(8,128)S(1)} %fusion.267) | copy-start | bytes 196612
  12.4 24.1 %copy-start.35 = (pred[128,128]{1,0:T(8,128)(4,1)}, pred[128,128]{1,0:T(8,128)(4,1)S(1)}, u32[]{:S(2)}) copy-start(pred[128,128]{1,0:T(8,128)(4,1)S(1)} %get-tuple-element.693) | copy-start | bytes 49156
  265.8 328.0 %all-gather.13.cloned.1.call-start = ((), (), s32[]{:S(2)}) async-start(), calls=%async_computation.6 | async-start | bytes 4325376 | tf_op jit(solution)/shard_map/all_gather | solution.py:44
  436.3 5.0 copy-start.10
  436.3 5.0 copy-start.11
  440.4 4.1 copy-start.4
  483.0 3.2 copy-start.21
  483.1 18.1 %copy-start.23 = (bf16[4,128,128]{2,1,0:T(8,128)(2,1)}, bf16[4,128,128]{2,1,0:T(8,128)(2,1)S(1)}, u32[]{:S(2)}) copy-start(bf16[4,128,128]{2,1,0:T(8,128)(2,1)S(1)} %fusion.287) | copy-start | bytes 393220
  486.3 0.6 copy-start.30
  487.2 0.7 copy-start.13
  514.3 1.4 copy-start.1
  514.5 2.1 copy-start.17
  514.7 1.9 copy-start.25
  514.9 1.7 copy-start.27
  514.9 8.5 copy-start.41
  523.4 31.1 %copy-start.22 = (bf16[4,128,128]{2,1,0:T(8,128)(2,1)S(1)}, bf16[4,128,128]{2,1,0:T(8,128)(2,1)}, u32[]{:S(2)}) copy-start(bf16[4,128,128]{2,1,0:T(8,128)(2,1)} %copy-done.21) | copy-start | bytes 393220
  523.4 31.1 %copy-start.24 = (bf16[4,128,128]{2,1,0:T(8,128)(2,1)S(1)}, bf16[4,128,128]{2,1,0:T(8,128)(2,1)}, u32[]{:S(2)}) copy-start(bf16[4,128,128]{2,1,0:T(8,128)(2,1)} %copy-done.23) | copy-start | bytes 393220
  523.4 31.9 %copy-start.18 = (bf16[4,128,128]{2,1,0:T(8,128)(2,1)S(1)}, bf16[4,128,128]{2,1,0:T(8,128)(2,1)}, u32[]{:S(2)}) copy-start(bf16[4,128,128]{2,1,0:T(8,128)(2,1)} %copy-done.17) | copy-start | bytes 393220
  523.4 31.9 %copy-start.19 = (bf16[4,128,128]{2,1,0:T(8,128)(2,1)S(1)}, bf16[4,128,128]{2,1,0:T(8,128)(2,1)}, u32[]{:S(2)}) copy-start(bf16[4,128,128]{2,1,0:T(8,128)(2,1)} %convolution_add_fusion.10) | copy-start | bytes 393220
  523.4 31.9 %copy-start.26 = (bf16[4,128,128]{2,1,0:T(8,128)(2,1)S(1)}, bf16[4,128,128]{2,1,0:T(8,128)(2,1)}, u32[]{:S(2)}) copy-start(bf16[4,128,128]{2,1,0:T(8,128)(2,1)} %copy-done.25) | copy-start | bytes 393220
  523.4 31.9 %copy-start.28 = (bf16[4,128,128]{2,1,0:T(8,128)(2,1)S(1)}, bf16[4,128,128]{2,1,0:T(8,128)(2,1)}, u32[]{:S(2)}) copy-start(bf16[4,128,128]{2,1,0:T(8,128)(2,1)} %copy-done.27) | copy-start | bytes 393220
  538.9 1.1 copy-start.14
  540.1 1.1 copy-start.15
  541.2 13.2 %copy-start.16 = (bf16[4,128,128]{2,1,0:T(8,128)(2,1)}, bf16[4,128,128]{2,1,0:T(8,128)(2,1)S(1)}, u32[]{:S(2)}) copy-start(bf16[4,128,128]{2,1,0:T(8,128)(2,1)S(1)} %fusion.290) | copy-start | bytes 393220
  554.6 0.6 copy-start.20
  559.1 7.3 copy-start.3
  559.1 7.3 copy-start.9
  663.6 2.2 copy-start.5
  663.6 2.2 copy-start.6
  663.6 2.5 copy-start.12
  676.1 5.0 copy-start.37
  676.1 6.6 copy-start.36
  676.1 43.6 %all-to-all-start = ((bf16[4,128,4096]{2,1,0:T(8,128)(2,1)}), bf16[4,128,4096]{2,1,0:T(8,128)(2,1)}, u32[]{:S(2)}, u32[]{:S(2)}) async-start(bf16[4,128,4096]{2,1,0:T(8,128)(2,1)} %bitcast.436), calls=%async_computation | async-start | bytes 8388608 | tf_op jit(solution)/shard_map/all_to_all | solution.py:73
  681.0 442.6 %reduce-scatter.2.cloned.1.call-start = ((), (), s32[]{:S(2)}) async-start(), calls=%async_computation.4 | async-start | bytes 15728640 | tf_op jit(solution)/shard_map/reduce_scatter | solution.py:279
  719.7 3.3 copy-start.29
  723.4 1.0 copy-start.7
  736.9 201.3 %copy-start.40 = (bf16[1,4096,384]{2,1,0:T(8,128)(2,1)S(1)}, bf16[1,4096,384]{2,1,0:T(8,128)(2,1)}, u32[]{:S(2)}) copy-start(bf16[1,4096,384]{2,1,0:T(8,128)(2,1)} %param.43) | copy-start | bytes 9437188
  932.5 5.7 copy-start.2
  1129.4 7.5 copy-start.39
  1129.4 61.5 %all-to-all-start.2 = ((bf16[32,1,1,12,4096]{4,3,2,1,0:T(8,128)(2,1)}), bf16[32,1,1,12,4096]{4,3,2,1,0:T(8,128)(2,1)}, u32[]{:S(2)}, u32[]{:S(2)}) async-start(bf16[32,1,1,12,4096]{4,3,2,1,0:T(8,128)(2,1)} %copy.388), calls=%async_computation.3 | async-start | bytes 8388608 | tf_op jit(solution)/shard_map/all_to_all | solution.py:287
  1196.4 3.6 copy-start.8
Sparse Core Ops, SparseCore 0:
  265.9 49.2 all-gather.10
  317.5 45.5 all-gather.12
  1014.0 109.6 reduce-scatter.1
where the time goes:
time: 1220 us; the launch traced here: 1210 us
  other arithmetic  352 us (29%)
  blocking collectives  254 us (21%)
  matrix products  209 us (17%)
  waiting for transfers between devices  201 us (16%)
  local copies, waits for them, and re-layouts  164 us (13%)
  between operations  14.2 us (1%)
  starting transfers between devices  12.8 us (1%)
    another operation x5, other arithmetic, prepare(): lax.linalg.triangular_solve(lower_mat, value_blk * beta_blk[..., None], l...  317 us
    all_to_all x1, blocking collectives, per_device(): lax.all_to_all(copies, SP_TP, split_axis=0, concat_axis=0, tiled=True)  196 us
    reduce_scatter x1, waiting for transfers between devices, per_device(): lax.psum_scatter(partial_value.reshape(sp_count, tp_count, exp_dev, capac...  110 us
    all_gather x6, blocking collectives, entering(): lax.all_gather(part.astype(kind), axis)  58 us
    all_to_all x1, waiting for transfers between devices, per_device(): lax.all_to_all(summed, SP, split_axis=0, concat_axis=0, tiled=True)  53.9 us
    dot_general x45, matrix products, combine(): jnp.einsum('hij,hjk->hik', later_pair[0], earlier_pair[1]) + later_pair[1]  44.9 us
    all_to_all x1, waiting for transfers between devices, summed_on_arrival(): lax.all_to_all(parts, axis, split_axis=0, concat_axis=0, tiled=True)  36.9 us
    rev x8, local copies, waits for them, and re-layouts, reverse_tokens(): return jnp.flip(tensor, axis=1)  35.9 us
  transfers between devices with their start and end apart: 5, of which 3 were waited for; matrix products, arithmetic and copies ran while one was open for 22% of the time, Pallas kernels for 0%

commit v1 on v0

v1 whole, which is shorter than its diff:
```python
import jax
import jax.numpy as jnp
from jax import lax
from jax.experimental import pallas as pl
from jax.experimental.pallas import tpu as pltpu
from jax.sharding import Mesh
from jax.sharding import PartitionSpec as P

HEAD_DIM = 128
TOPK = 2
BLOCK = 128
SP = ("sp_0", "sp_1", "sp_2")
SP_TP = ("sp_0", "sp_1", "sp_2", "tp")
ARB = pltpu.CompilerParams(dimension_semantics=("arbitrary",), vmem_limit_bytes=48 * 1024 * 1024)
MESH = pl.DeviceIdType.MESH
NBLK = 4
f32 = jnp.float32
bf16 = jnp.bfloat16


def mm(a, b):
    return jnp.dot(a, b, preferred_element_type=f32)


def local_kernel(q_ref, k_ref, v_ref, ld_ref, bt_ref, out_ref, qeff_ref, blk_ref, comp_ref):
    n = BLOCK
    row = lax.broadcasted_iota(jnp.int32, (n, n), 0)
    col = lax.broadcasted_iota(jnp.int32, (n, n), 1)
    upper = (row <= col).astype(f32)
    lower = (row >= col).astype(f32)
    eye = (row == col).astype(f32)
    ld = ld_ref[0]
    highest = lax.Precision.HIGHEST
    run_f = jnp.dot(ld, upper, precision=highest, preferred_element_type=f32)
    run_b = jnp.dot(ld, lower, precision=highest, preferred_element_type=f32)
    which = lax.broadcasted_iota(jnp.int32, (2 * NBLK, n), 0)
    cum_rows = jnp.where(which < NBLK, run_f, run_b)
    cum_cols = jnp.transpose(cum_rows)
    beta_cols = jnp.transpose(bt_ref[0])
    chains = [(d, b) for d in range(2) for b in range(NBLK)]
    grams, k_un, v_un, q_un, kt_un = [], [], [], [], []
    for b in range(NBLK):
        rows = pl.ds(b * n, n)
        q = q_ref[rows, :].astype(f32)
        k = k_ref[rows, :].astype(f32)
        q = q * lax.rsqrt(jnp.sum(q * q, axis=-1, keepdims=True) + 1e-06) * HEAD_DIM ** (-0.5)
        k = k * lax.rsqrt(jnp.sum(k * k, axis=-1, keepdims=True) + 1e-06)
        kt = jnp.transpose(k).astype(bf16)
        grams.append((mm(k.astype(bf16), kt), mm(q.astype(bf16), kt)))
        q_un.append(q)
        k_un.append(k)
        kt_un.append(kt)
        v_un.append(v_ref[rows, :].astype(f32))
    low, attn, sums, pows = {}, {}, {}, {}
    for d, b in chains:
        i = d * NBLK + b
        gap = cum_cols[:, i : i + 1] - cum_rows[i : i + 1, :]
        keep = row >= col if d == 0 else row <= col
        decay = jnp.exp(jnp.where(keep, gap, -1e30))
        attn[d, b] = (grams[b][1] * decay).astype(bf16)
        strict = row > col if d == 0 else row < col
        low = jnp.where(strict, grams[b][0] * decay, 0.0) * beta_cols[:, i : i + 1]
        sums[d, b] = eye - low
        pows[d, b] = low.astype(bf16)
    for c in chains:
        pows[c] = mm(pows[c], pows[c]).astype(bf16)
    for step in range(5):
        for c in chains:
            both = mm(jnp.concatenate([sums[c].astype(bf16), pows[c]], axis=0), pows[c])
            sums[c] = sums[c] + both[:n]
            pows[c] = both[n:].astype(bf16)
    for c in chains:
        sums[c] = sums[c] + mm(sums[c].astype(bf16), pows[c])
    fresh, maps = {}, {}
    for d, b in chains:
        i = d * NBLK + b
        cc = cum_cols[:, i : i + 1]
        bt = beta_cols[:, i : i + 1]
        right = jnp.concatenate([v_un[b] * bt, k_un[b] * (-bt * jnp.exp(cc))], axis=1)
        fresh[d, b] = mm(sums[d, b].astype(bf16), right.astype(bf16))
    for d, b in chains:
        i = d * NBLK + b
        cc = cum_cols[:, i : i + 1]
        last = n - 1 if d == 0 else 0
        total = cum_rows[i : i + 1, last : last + 1]
        ended = (fresh[d, b] * jnp.exp(total - cc)).astype(bf16)
        step_map = mm(kt_un[b], ended) + jnp.concatenate(
            [jnp.zeros((n, n), f32), eye * jnp.exp(total)], axis=1
        )
        maps[d, b] = step_map
        blk_ref[0, i] = step_map.astype(bf16)
    for b in range(NBLK):
        rows = pl.ds(b * n, n)
        locals_, effs = [], []
        for d in range(2):
            i = d * NBLK + b
            given = mm(attn[d, b], fresh[d, b].astype(bf16))
            locals_.append(given[:, :n])
            effs.append(given[:, n:] + q_un[b] * jnp.exp(cum_cols[:, i : i + 1]))
        out_ref[rows, :] = locals_[0] + locals_[1]
        qeff_ref[0, rows, :] = jnp.concatenate(effs, axis=1).astype(bf16)

    def after(later, earlier):
        moved = mm(later[:, n:].astype(bf16), earlier.astype(bf16))
        return jnp.concatenate([moved[:, :n] + later[:, :n], moved[:, n:]], axis=1)

    for d in range(2):
        order = range(NBLK) if d == 0 else range(NBLK - 1, -1, -1)
        first, second, third, fourth = [maps[d, b] for b in order]
        comp_ref[0, d] = after(after(fourth, third), after(second, first)).astype(bf16)


def local_pass(queries, keys, values, log_decay, beta, heads):
    tok = queries.shape[0]
    n = BLOCK
    columns = pl.BlockSpec((tok, n), lambda h: (0, h))
    small = pl.BlockSpec((1, 2 * NBLK, n), lambda h: (h, 0, 0))
    return pl.pallas_call(
        local_kernel,
        grid=(heads,),
        in_specs=[columns, columns, columns, small, small],
        out_specs=[
            columns,
            pl.BlockSpec((1, tok, 2 * n), lambda h: (h, 0, 0)),
            pl.BlockSpec((1, 2 * NBLK, n, 2 * n), lambda h: (h, 0, 0, 0)),
            pl.BlockSpec((1, 2, n, 2 * n), lambda h: (h, 0, 0, 0)),
        ],
        out_shape=[
            jax.ShapeDtypeStruct((tok, heads * n), f32),
            jax.ShapeDtypeStruct((heads, tok, 2 * n), bf16),
            jax.ShapeDtypeStruct((heads, 2 * NBLK, n, 2 * n), bf16),
            jax.ShapeDtypeStruct((heads, 2, n, 2 * n), bf16),
        ],
        compiler_params=ARB,
        name="local_pass",
    )(queries, keys, values, log_decay, beta)


def exchange_kernel(comp_ref, out_ref, got, pre, chunk, start, ready, send1, recv1, send2, recv2):
    n = BLOCK
    z, y, core = (lax.axis_index(a) for a in SP)
    me = (z * 4 + y) * 2 + core
    is_owner = jnp.logical_and(core == 1, y % 2 == z % 2)
    way = y // 2
    mine = z * 2 + way

    def place(s):
        return {"sp_0": s // 8, "sp_1": (s // 2) % 4, "sp_2": s % 2}

    barrier = pltpu.get_barrier_semaphore()

    def greet(i, carry):
        other = (me + i) % 32
        pl.semaphore_signal(barrier, inc=1, device_id=place(other), device_id_type=MESH)
        return carry

    lax.fori_loop(1, 32, greet, 0)
    pl.semaphore_wait(barrier, 31)

    def owner_of(c):
        oz = c // 2
        return (oz * 4 + (c % 2) * 2 + oz % 2) * 2 + 1

    def first_copy(c):
        return pltpu.make_async_remote_copy(
            src_ref=comp_ref.at[c],
            dst_ref=got.at[me],
            send_sem=send1.at[c],
            recv_sem=recv1.at[me],
            device_id=place(owner_of(c)),
            device_id_type=MESH,
        )

    for c in range(8):
        own = owner_of(c)

        @pl.when(me != own)
        def _():
            first_copy(c).start()

        @pl.when(me == own)
        def _():
            got[me] = comp_ref[c]

    def arrival(s):
        return pltpu.make_async_remote_copy(
            src_ref=comp_ref.at[0],
            dst_ref=got.at[s],
            send_sem=send1.at[0],
            recv_sem=recv1.at[s],
            device_id=place(s),
            device_id_type=MESH,
        )

    def second_copy(p, s):
        return pltpu.make_async_remote_copy(
            src_ref=ready.at[p],
            dst_ref=out_ref.at[mine],
            send_sem=send2.at[p],
            recv_sem=recv2.at[mine],
            device_id=place(s),
            device_id_type=MESH,
        )

    @pl.when(is_owner)
    def _():
        row = lax.broadcasted_iota(jnp.int32, (n, 2 * n), 0)
        col = lax.broadcasted_iota(jnp.int32, (n, 2 * n), 1)
        unit = (row + n == col).astype(f32)
        for j in range(4):
            chunk[j] = unit

        def step(r, carry):
            for j in range(4):
                p = 8 * j + r
                s = p + way * (31 - 2 * p)

                @pl.when(s != me)
                def _():
                    arrival(s).wait_recv()

                now = chunk[j].astype(bf16)
                pre[p] = now
                moved = mm(got[s, :, n:], now)
                chunk[j, :, :n] = moved[:, :n] + got[s, :, :n].astype(f32)
                chunk[j, :, n:] = moved[:, n:]
            return carry

        lax.fori_loop(0, 8, step, 0)
        start[0] = jnp.zeros((n, n), bf16)
        held = jnp.zeros((n, n), f32)
        for j in range(3):
            held = mm(chunk[j, :, n:].astype(bf16), held.astype(bf16)) + chunk[j, :, :n]
            start[j + 1] = held.astype(bf16)

        def finish(r, carry):
            for j in range(4):
                p = 8 * j + r
                s = p + way * (31 - 2 * p)
                given = mm(pre[p, :, n:], start[j]) + pre[p, :, :n].astype(f32)
                ready[p] = given.astype(bf16)

                @pl.when(s != me)
                def _():
                    second_copy(p, s).start()

                @pl.when(s == me)
                def _():
                    out_ref[mine] = given.astype(bf16)

            return carry

        lax.fori_loop(0, 8, finish, 0)

        def drain(p, carry):
            s = p + way * (31 - 2 * p)

            @pl.when(s != me)
            def _():
                second_copy(p, s).wait_send()

            return carry

        lax.fori_loop(0, 32, drain, 0)

    for c in range(8):

        @pl.when(me != owner_of(c))
        def _():
            first_copy(c).wait_send()
            pltpu.make_async_remote_copy(
                src_ref=ready.at[0],
                dst_ref=out_ref.at[c],
                send_sem=send2.at[0],
                recv_sem=recv2.at[c],
                device_id=place(owner_of(c)),
                device_id_type=MESH,
            ).wait_recv()


def exchange(comp):
    n = BLOCK
    return pl.pallas_call(
        exchange_kernel,
        in_specs=[pl.BlockSpec(memory_space=pltpu.VMEM)],
        out_specs=pl.BlockSpec(memory_space=pltpu.VMEM),
        out_shape=jax.ShapeDtypeStruct((8, n, n), bf16),
        scratch_shapes=[
            pltpu.VMEM((32, n, 2 * n), bf16),
            pltpu.VMEM((32, n, 2 * n), bf16),
            pltpu.VMEM((4, n, 2 * n), f32),
            pltpu.VMEM((4, n, n), bf16),
            pltpu.VMEM((32, n, n), bf16),
            pltpu.SemaphoreType.DMA((8,)),
            pltpu.SemaphoreType.DMA((32,)),
            pltpu.SemaphoreType.DMA((32,)),
            pltpu.SemaphoreType.DMA((8,)),
        ],
        compiler_params=pltpu.CompilerParams(collective_id=0, has_side_effects=True),
        name="exchange",
    )(comp)


def finish_kernel(out_ref, qeff_ref, blk_ref, sin_ref, gate_ref, gain_ref, mix_ref):
    n = BLOCK
    gain = gain_ref[...].astype(f32)
    states = {}
    held = [sin_ref[0, d].astype(f32) for d in range(2)]
    for step in range(NBLK):
        for d in range(2):
            b = step if d == 0 else NBLK - 1 - step
            states[d, b] = held[d].astype(bf16)
            if step < NBLK - 1:
                i = d * NBLK + b
                held[d] = mm(blk_ref[0, i, :, n:], states[d, b]) + blk_ref[0, i, :, :n].astype(f32)
    for b in range(NBLK):
        rows = pl.ds(b * n, n)
        both = jnp.concatenate([states[0, b], states[1, b]], axis=0)
        o = out_ref[rows, :] + mm(qeff_ref[0, rows, :], both)
        o = o * lax.rsqrt(jnp.mean(o * o, axis=-1, keepdims=True) + 1e-06) * gain
        g = gate_ref[rows, :].astype(f32)
        mix_ref[rows, :] = (o * (g * jax.nn.sigmoid(g))).astype(bf16)


def finish_pass(out_local, qeff, blk, entering, gates, gain):
    tok, width = out_local.shape
    n = BLOCK
    heads = width // n
    columns = pl.BlockSpec((tok, n), lambda h: (0, h))
    return pl.pallas_call(
        finish_kernel,
        grid=(heads,),
        in_specs=[
            columns,
            pl.BlockSpec((1, tok, 2 * n), lambda h: (h, 0, 0)),
            pl.BlockSpec((1, 2 * NBLK, n, 2 * n), lambda h: (h, 0, 0, 0)),
            pl.BlockSpec((1, 2, n, n), lambda h: (h, 0, 0, 0)),
            columns,
            pl.BlockSpec((1, n), lambda h: (0, 0)),
        ],
        out_specs=columns,
        out_shape=jax.ShapeDtypeStruct((tok, width), bf16),
        compiler_params=ARB,
        name="finish_pass",
    )(out_local, qeff, blk, entering, gates, gain)


def head_mixing(queries, keys, values, gates, decay_logits, write_logits, extra, rate, gain):
    tok, width = queries.shape
    heads = width // HEAD_DIM
    log_decay = -rate[:, None, :] * jax.nn.softplus(decay_logits) + extra
    beta = jax.nn.sigmoid(write_logits)

    def per_head(t):
        t = t.transpose(2, 0, 1).reshape(heads, 2 * NBLK, BLOCK)
        return t

    out_local, qeff, blk, comp = local_pass(
        queries, keys, values, per_head(log_decay), per_head(beta), heads
    )
    entering = exchange(comp.reshape(2 * heads, BLOCK, 2 * BLOCK))
    return finish_pass(
        out_local, qeff, blk, entering.reshape(heads, 2, BLOCK, BLOCK), gates, gain.reshape(1, -1)
    )


def in_blocks(shard, dim, count):
    shape = shard.shape
    parts = shard.reshape(*shape[:dim], count, shape[dim] // count, *shape[dim + 1 :])
    return jnp.moveaxis(parts, dim, 0)


def summed_on_arrival(shard, axis, dim):
    parts = in_blocks(shard, dim, lax.axis_size(axis))
    arrived = lax.all_to_all(parts, axis, split_axis=0, concat_axis=0, tiled=True)
    return arrived.astype(jnp.float32).sum(axis=0)


def per_device(
    queries,
    keys,
    values,
    output_gate_logits,
    decay_gate_logits,
    write_strength_logits,
    extra_log_decay,
    head_decay_rate,
    head_norm_gain,
    output_weight,
    residual,
    expert_norm_gain,
    selected_experts,
    router_chosen_scores,
    gate_up_weight,
    linear_up_weight,
    down_weight,
):
    tok_rows, width_dev = queries.shape
    head_mix = head_mixing(
        queries,
        keys,
        values,
        output_gate_logits,
        decay_gate_logits,
        write_strength_logits,
        extra_log_decay,
        head_decay_rate,
        head_norm_gain,
    )
    local_rows = residual.shape[0]
    mix_sum = summed_on_arrival(
        jnp.dot(head_mix, output_weight, preferred_element_type=jnp.float32).astype(jnp.bfloat16),
        "tp",
        0,
    )
    stream = (residual.astype(jnp.float32) + mix_sum).astype(jnp.bfloat16)
    stream_wide = stream.astype(jnp.float32)
    normed = (
        stream_wide
        * lax.rsqrt(jnp.mean(stream_wide * stream_wide, axis=-1, keepdims=True) + 1e-06)
        * expert_norm_gain.astype(jnp.float32)
    ).astype(jnp.bfloat16)
    route_exp = jnp.exp(router_chosen_scores)
    route_weight = route_exp / jnp.sum(route_exp, axis=-1, keepdims=True)
    sp_count = lax.axis_size(SP)
    tp_count = lax.axis_size("tp")
    exp_dev = gate_up_weight.shape[0]
    experts = exp_dev * sp_count
    capacity = 3 * TOPK * tok_rows // (2 * tp_count * experts)
    model_width = normed.shape[1]
    flat_experts = selected_experts.reshape(-1)
    member = (flat_experts[:, None] == jnp.arange(experts, dtype=jnp.int32)[None, :]).astype(
        jnp.int32
    )
    slot_rank = jnp.sum(jnp.cumsum(member, axis=0) * member, axis=1) - 1
    slot_index = flat_experts * capacity + slot_rank
    slot_hot = (
        slot_index[:, None] == jnp.arange(experts * capacity, dtype=jnp.int32)[None, :]
    ).astype(jnp.bfloat16)
    token_hot = jnp.sum(slot_hot.reshape(local_rows, TOPK, experts * capacity), axis=1)
    outgoing = jnp.einsum(
        "rs,rd->sd", token_hot, normed, preferred_element_type=jnp.float32
    ).astype(jnp.bfloat16)
    grouped = outgoing.reshape(sp_count, exp_dev, capacity, model_width)
    copies = jnp.broadcast_to(
        grouped[:, None], (sp_count, tp_count, exp_dev, capacity, model_width)
    )
    copies = copies.reshape(sp_count * tp_count, exp_dev, capacity, model_width)
    arrived = lax.all_to_all(copies, SP_TP, split_axis=0, concat_axis=0, tiled=True)
    gate_pre = jnp.einsum(
        "secd,edf->secf", arrived, gate_up_weight, preferred_element_type=jnp.float32
    )
    linear_pre = jnp.einsum(
        "secd,edf->secf", arrived, linear_up_weight, preferred_element_type=jnp.float32
    )
    clipped = jnp.minimum(gate_pre, 7.0)
    hidden_act = (
        clipped * jax.nn.sigmoid(1.702 * clipped) * (jnp.clip(linear_pre, -7.0, 7.0) + 1.0)
    ).astype(jnp.bfloat16)
    partial_value = jnp.einsum(
        "secf,efd->secd", hidden_act, down_weight, preferred_element_type=jnp.float32
    )
    summed = lax.psum_scatter(
        partial_value.reshape(sp_count, tp_count, exp_dev, capacity, model_width).astype(
            jnp.bfloat16
        ),
        "tp",
        scatter_dimension=1,
        tiled=True,
    )
    returned = lax.all_to_all(summed, SP, split_axis=0, concat_axis=0, tiled=True)
    returned = returned.reshape(experts * capacity, model_width)
    picked = jnp.dot(slot_hot, returned, preferred_element_type=jnp.float32).reshape(
        local_rows, TOPK, model_width
    )
    combined = jnp.sum(picked * route_weight[:, :, None], axis=1)
    return (stream_wide + combined).astype(jnp.bfloat16)


def solution(mesh):
    torus = Mesh(mesh.devices.reshape(4, 4, 2, mesh.shape["tp"]), ("sp_0", "sp_1", "sp_2", "tp"))
    placed = (
        P(SP, "tp"),
        P(SP, "tp"),
        P(SP, "tp"),
        P(SP, "tp"),
        P(None, SP, "tp"),
        P(None, SP, "tp"),
        P(None, SP, "tp"),
        P(None, "tp"),
        P(),
        P("tp", None),
        P(SP_TP, None),
        P(),
        P(SP_TP, None),
        P(SP_TP, None),
        P(SP, None, "tp"),
        P(SP, None, "tp"),
        P(SP, "tp", None),
    )
    return jax.shard_map(
        per_device, mesh=torus, in_specs=placed, out_specs=P(SP_TP, None), check_vma=False
    )
```

time: 1220 us -> 629 us (0.52)
  other arithmetic: 352 us -> 8.29 us
  matrix products: 209 us -> 52.9 us
  local copies, waits for them, and re-layouts: 164 us -> 74.8 us
  blocking collectives: 254 us -> 196 us
  Pallas kernels: 0 us -> 51.5 us
    another operation x9 -> x2, other arithmetic: 320 us -> 0.63 us  [the longest x5 317 us: prepare(): lax.linalg.triangular_solve(lower_mat, value_blk * beta_blk[..., None], l...]
    dot_general x104 -> x0, matrix products: 140 us -> none  [the longest x45 44.9 us: combine(): jnp.einsum('hij,hjk->hik', later_pair[0], earlier_pair[1]) + later_pair[1]]
    all_gather x6 -> x0, blocking collectives: 58 us -> none  [entering(): lax.all_gather(part.astype(kind), axis)]
    pallas_call x0 -> x3, Pallas kernels: none -> 51.5 us  [the longest x1 36.1 us: exchange(): pl.pallas_call(exchange_kernel, in_specs=[pl.BlockSpec(memory_space=pltpu...]
    rev x8 -> x0, local copies, waits for them, and re-layouts: 35.9 us -> none  [reverse_tokens(): return jnp.flip(tensor, axis=1)]
    while x48 -> x0, local copies, waits for them, and re-layouts: 21.6 us -> none
    another operation x4 -> x0, matrix products: 13.8 us -> none  [the longest x2 8 us: prepare(): lax.linalg.triangular_solve(lower_mat, key_beta * jnp.exp(cumulative)[......]
    unnamed x97 -> x47, local copies, waits for them, and re-layouts: 25.3 us -> 19.4 us
  transfers between devices with their start and end apart: 5 -> 3, of which waited for: 3 -> 3; matrix products, arithmetic and copies ran while one was open for 22% -> 0% of each run, Pallas kernels for 0% -> 0%
where the time goes in v1:
time: 629 us; the launch traced here: 620 us
  waiting for transfers between devices  210 us (33%)
  blocking collectives  196 us (31%)
  local copies, waits for them, and re-layouts  74.8 us (12%)
  matrix products  52.9 us (8%)
  Pallas kernels  51.5 us (8%)
  between operations  14.1 us (2%)
  starting transfers between devices  12.5 us (2%)
  other arithmetic  8.29 us (1%)
    all_to_all x1, blocking collectives, per_device(): lax.all_to_all(copies, SP_TP, split_axis=0, concat_axis=0, tiled=True)  196 us
    reduce_scatter x1, waiting for transfers between devices, per_device(): lax.psum_scatter(partial_value.reshape(sp_count, tp_count, exp_dev, capac...  110 us
    all_to_all x1, waiting for transfers between devices, per_device(): lax.all_to_all(summed, SP, split_axis=0, concat_axis=0, tiled=True)  53.9 us
    all_to_all x1, waiting for transfers between devices, summed_on_arrival(): lax.all_to_all(parts, axis, split_axis=0, concat_axis=0, tiled=True)  46.3 us
    pallas_call x1, Pallas kernels, exchange(): pl.pallas_call(exchange_kernel, in_specs=[pl.BlockSpec(memory_space=pltpu...  36.1 us
    convert_element_type x2, local copies, waits for them, and re-layouts, per_device(): partial_value.reshape(sp_count, tp_count, exp_dev, capacity, model_width)  33.7 us
    dot_general x1, matrix products, per_device(): jnp.einsum('secf,efd->secd', hidden_act, down_weight, preferred_element_t...  25.9 us
    unnamed x47, local copies, waits for them, and re-layouts  19.4 us
  transfers between devices with their start and end apart: 3, of which 3 were waited for; matrix products, arithmetic and copies ran while one was open for 0% of the time, Pallas kernels for 0%

profile of v1, /device:TPU:0, one launch (start us, length us, event | category | flops | bytes accessed | tf_op | source)
XLA Modules:
  0.0 619.7 jit_solution(108452494995952406)
XLA Ops:
  6.5 0.0 copy-start
  6.5 0.8 neg.14
  7.4 0.9 fusion.45
  8.3 0.7 divide_bitcast_fusion
  9.1 0.0 copy-start.8
  9.1 1.0 copy-done.8
  10.2 1.0 copy-done.9
  11.2 1.0 copy-done.10
  12.2 12.1 %local_pass.1 = (f32[512,512]{1,0:T(8,128)S(1)}, bf16[4,512,256]{2,1,0:T(8,128)(2,1)S(1)}, bf16[4,8,128,256]{3,2,1,0:T(8,128)(2,1)}, bf16[4,2,128,256]{3,2,1,0:T(8,128)(2,1)S(1)}) custom-call(bf16[512,512]{1,0:T(8,128)(2,1)S(1)} %copy-done.8, bf16[512,512]{1,0:T(8,128)(2,1)S(1)} %copy-done.9, bf16[512,512]{1,0:T(8,128)(2,1)S(1)} %copy-done.10, ...), custom_call_target="tpu_custom_call" | custom-call | tf_op jit(solution)/shard_map/local_pass/pallas_call | solution.py:118
  24.3 1.0 copy-done.4
  25.3 1.0 copy-done.6
  26.3 0.8 copy-done.11
  27.1 36.1 %exchange.1 = bf16[8,128,128]{2,1,0:T(8,128)(2,1)} custom-call(bf16[8,128,256]{2,1,0:T(8,128)(2,1)} %bitcast.110), custom_call_target="tpu_custom_call" | custom-call | tf_op jit(solution)/shard_map/exchange/pallas_call | solution.py:283
  63.2 0.0 copy-start.2
  63.2 1.6 copy-done.2
  64.8 0.9 copy-done.3
  65.8 1.2 copy-done.5
  67.0 1.2 copy-done.7
  68.2 1.0 copy-done.12
  69.3 0.7 copy-done.13
  69.9 3.3 finish_pass.1
  73.2 0.0 copy-done.21
  73.2 4.4 convolution_convert_fusion
  77.6 5.0 all-to-all-start
  82.6 0.0 reduce-scatter.2.cloned.1.call-start
  82.7 0.0 copy-done.19
  82.7 0.1 copy.68
  82.8 0.1 eq.65
  82.9 0.1 eq.61
  83.1 0.6 reduce-window.6
  83.7 0.2 slice_reduce_fusion
  83.9 0.1 fusion.41
  84.0 0.1 sub.7
  84.2 0.1 copy.71
  84.2 0.0 copy-done.18
  84.3 0.1 fusion.38
  84.4 46.3 %all-to-all-done = bf16[4,128,4096]{2,1,0:T(8,128)(2,1)} async-done(((bf16[4,128,4096]{2,1,0:T(8,128)(2,1)}), bf16[4,128,4096]{2,1,0:T(8,128)(2,1)}, u32[]{:S(2)}, u32[]{:S(2)}) %all-to-all-start) | async-done | bytes 4194336 | tf_op jit(solution)/shard_map/all_to_all | solution.py:375
  130.7 3.3 convert_reduce_fusion
  134.0 0.0 copy-done.17
  134.0 0.4 fusion.14
  134.4 0.0 copy-start.15
  134.4 1.0 copy-done.15
  135.4 2.8 convolution_convert_fusion.1
  138.1 5.5 broadcast_in_dim.6
  143.6 4.2 broadcast_in_dim.7
  147.9 0.0 copy-start.22
  147.9 195.6 %all_to_all.15 = bf16[128,1,12,4096]{3,2,1,0:T(8,128)(2,1)S(1)} all-to-all(bf16[128,1,12,4096]{3,2,1,0:T(8,128)(2,1)S(1)} %bitcast.112), channel_id=1, replica_groups=mesh['sp_0'=4,'sp_1'=4,'sp_2'=2,'tp'=4] {'sp_0','sp_1','sp_2','tp'}, dimensions={0} | all-to-all | bytes 25165824 | tf_op jit(solution)/shard_map/all_to_all | solution.py:449
  343.5 5.7 copy-done.14
  349.2 0.0 copy-done.22
  349.2 16.1 %fusion.2 = f32[128,12,384]{2,0,1:T(8,128)} fusion(bf16[128,1,12,4096]{3,2,1,0:T(8,128)(2,1)S(1)} %all_to_all.15, bf16[1,4096,384]{2,1,0:T(8,128)(2,1)S(1)} %copy-done.22), kind=kOutput, calls=%fused_computation.2 | convolution fusion | flops 4831838208 | bytes 18087936 | tf_op jit(solution)/shard_map/secd,edf->secf/dot_general | solution.py:450
  365.4 0.0 copy-done
  365.4 25.9 %convert_bitcast_fusion = bf16[128,1,12,4096]{3,0,2,1:T(8,128)(2,1)} fusion(bf16[1,384,4096]{2,1,0:T(8,128)(2,1)S(1)} %copy-done, bf16[1,4096,384]{2,1,0:T(8,128)(2,1)} %param.32, bf16[128,1,12,4096]{3,2,1,0:T(8,128)(2,1)} %copy-done.14, f32[128,12,384]{2,0,1:T(8,128)} %fusion.2), kind=kOutput, calls=%fused_computation.4 | convolution fusion | flops 9675866112 | bytes 33816576 | tf_op jit(solution)/shard_map/secf,efd->secd/dot_general | solution.py:460
  391.2 19.0 %convert_element_type.79 = bf16[32,4,1,12,4096]{4,1,0,3,2:T(4,128)(2,1)} reshape(bf16[128,1,12,4096]{3,0,2,1:T(8,128)(2,1)} %convert_bitcast_fusion) | data formatting | bytes 25165824 | tf_op jit(solution)/shard_map/convert_element_type | solution.py:464
  410.2 14.7 %copy.73 = bf16[32,4,1,12,4096]{4,0,3,2,1:T(8,128)(2,1)} copy(bf16[32,4,1,12,4096]{4,1,0,3,2:T(4,128)(2,1)} %convert_element_type.79) | data formatting | bytes 25165824 | tf_op jit(solution)/shard_map/convert_element_type | solution.py:464
  424.9 0.0 reduce-scatter.2.cloned.1.call-update
  424.9 109.9 %reduce-scatter.2.cloned.1.call-done = bf16[32,1,1,12,4096]{4,0,3,2,1:T(8,128)(2,1)} async-done(((bf16[32,4,1,12,4096]{4,0,3,2,1:T(8,128)(2,1)}), bf16[32,1,1,12,4096]{4,0,3,2,1:T(8,128)(2,1)}) %reduce-scatter.2.cloned.1.call-update) | async-done | bytes 3145744 | tf_op jit(solution)/shard_map/reduce_scatter | solution.py:463
  534.8 5.7 copy.74
  540.4 7.5 %all-to-all-start.2 = ((bf16[32,1,1,12,4096]{4,3,2,1,0:T(8,128)(2,1)}), bf16[32,1,1,12,4096]{4,3,2,1,0:T(8,128)(2,1)}, u32[]{:S(2)}, u32[]{:S(2)}) async-start(bf16[32,1,1,12,4096]{4,3,2,1,0:T(8,128)(2,1)} %copy.74), calls=%async_computation.3 | async-start | bytes 8388608 | tf_op jit(solution)/shard_map/all_to_all | solution.py:471
  548.0 0.0 copy-done.20
  548.0 53.9 %all-to-all-done.2 = bf16[32,1,1,12,4096]{4,3,2,1,0:T(8,128)(2,1)} async-done(((bf16[32,1,1,12,4096]{4,3,2,1,0:T(8,128)(2,1)}), bf16[32,1,1,12,4096]{4,3,2,1,0:T(8,128)(2,1)}, u32[]{:S(2)}, u32[]{:S(2)}) %all-to-all-start.2) | async-done | bytes 3145760 | tf_op jit(solution)/shard_map/all_to_all | solution.py:471
  601.9 5.6 reshape.160
  607.5 3.7 fusion.18
  611.3 0.0 copy-done.16
  611.3 1.2 fusion.17
  (32 shorter events, 0.2 us)
Async XLA Ops:
  6.5 358.8 %copy-start = (bf16[1,384,4096]{2,1,0:T(8,128)(2,1)S(1)}, bf16[1,384,4096]{2,1,0:T(8,128)(2,1)}, u32[]{:S(2)}) copy-start(bf16[1,384,4096]{2,1,0:T(8,128)(2,1)} %param.33) | copy-start | bytes 9437188
  9.1 1.0 copy-start.8
  10.2 1.0 copy-start.9
  11.2 1.0 copy-start.10
  24.3 1.0 copy-start.4
  25.3 1.0 copy-start.6
  26.3 0.8 copy-start.11
  63.2 1.6 copy-start.2
  64.8 0.9 copy-start.3
  65.8 1.2 copy-start.5
  67.0 1.2 copy-start.7
  68.2 1.0 copy-start.12
  69.3 0.7 copy-start.13
  69.9 3.3 copy-start.21
  77.6 5.0 copy-start.19
  77.6 6.6 %copy-start.18 = (bf16[4096]{0:T(1024)(128)(2,1)S(1)}, bf16[4096]{0:T(1024)(128)(2,1)}, u32[]{:S(2)}) copy-start(bf16[4096]{0:T(1024)(128)(2,1)} %param.28) | copy-start | bytes 24580
  77.6 53.0 %all-to-all-start = ((bf16[4,128,4096]{2,1,0:T(8,128)(2,1)}), bf16[4,128,4096]{2,1,0:T(8,128)(2,1)}, u32[]{:S(2)}, u32[]{:S(2)}) async-start(bf16[4,128,4096]{2,1,0:T(8,128)(2,1)} %bitcast.113), calls=%async_computation | async-start | bytes 8388608 | tf_op jit(solution)/shard_map/all_to_all | solution.py:375
  82.6 452.2 %reduce-scatter.2.cloned.1.call-start = ((), (), s32[]{:S(2)}) async-start(), calls=%async_computation.4 | async-start | bytes 15728640 | tf_op jit(solution)/shard_map/reduce_scatter | solution.py:463
  130.7 3.3 copy-start.17
  134.4 1.0 copy-start.15
  147.9 201.3 %copy-start.22 = (bf16[1,4096,384]{2,1,0:T(8,128)(2,1)S(1)}, bf16[1,4096,384]{2,1,0:T(8,128)(2,1)}, u32[]{:S(2)}) copy-start(bf16[1,4096,384]{2,1,0:T(8,128)(2,1)} %param.31) | copy-start | bytes 9437188
  343.5 5.7 copy-start.14
  540.4 7.5 %copy-start.20 = (f32[128,2]{0,1:T(2,128)S(1)}, f32[128,2]{0,1:T(2,128)}, u32[]{:S(2)}) copy-start(f32[128,2]{0,1:T(2,128)} %param.30) | copy-start | bytes 3076
  540.4 61.5 %all-to-all-start.2 = ((bf16[32,1,1,12,4096]{4,3,2,1,0:T(8,128)(2,1)}), bf16[32,1,1,12,4096]{4,3,2,1,0:T(8,128)(2,1)}, u32[]{:S(2)}, u32[]{:S(2)}) async-start(bf16[32,1,1,12,4096]{4,3,2,1,0:T(8,128)(2,1)} %copy.74), calls=%async_computation.3 | async-start | bytes 8388608 | tf_op jit(solution)/shard_map/all_to_all | solution.py:471
  607.5 3.7 copy-start.16
  607.5 4.9 copy-start.1
Sparse Core Ops, SparseCore 0:
  425.0 109.6 reduce-scatter.1

commit v2 on v1

--- a/solution.py
+++ b/solution.py
@@ -376,6 +376,316 @@
     return arrived.astype(jnp.float32).sum(axis=0)
 
 
+PLANE = (
+    (0, 0), (0, 1), (1, 0), (0, 3), (3, 0), (1, 1), (3, 3), (1, 3),
+    (3, 1), (0, 2), (2, 0), (1, 2), (3, 2), (2, 1), (2, 3), (2, 2),
+)
+ORDER = tuple((dz, dy, dc) for dz, dy in PLANE for dc in range(2))
+CAP = 12
+SLOTS = len(ORDER)
+HALF = 2048
+FFD = 384
+ROWS = SLOTS * CAP
+
+
+def plane_place(z, y, core, offset, sign):
+    dz, dy, dc = offset
+    return {
+        "sp_0": lax.rem(z + (dz if sign > 0 else 4 - dz), 4),
+        "sp_1": lax.rem(y + (dy if sign > 0 else 4 - dy), 4),
+        "sp_2": lax.rem(core + dc, 2),
+    }
+
+
+def greet_all(z, y, core, x, around):
+    barrier = pltpu.get_barrier_semaphore()
+    for offset in ORDER[1:]:
+        pl.semaphore_signal(
+            barrier, inc=1, device_id=plane_place(z, y, core, offset, 1), device_id_type=MESH
+        )
+    count = SLOTS - 1
+    if around:
+        for dx in range(1, 4):
+            pl.semaphore_signal(
+                barrier, inc=1, device_id={"tp": lax.rem(x + dx, 4)}, device_id_type=MESH
+            )
+        count += 3
+    pl.semaphore_wait(barrier, count)
+
+
+def dispatch_kernel(
+    blocks_ref, gate_ref, lin_ref, hid_ref,
+    xb, wg, wl, rows_buf, act_buf,
+    wsem, send0, send1, send2, send3, recv, hsend, hrecv,
+):
+    z, y, core = (lax.axis_index(a) for a in SP)
+    x = lax.axis_index("tp")
+    right, left, far = lax.rem(x + 1, 4), lax.rem(x + 3, 4), lax.rem(x + 2, 4)
+    load_g = pltpu.make_async_copy(gate_ref, wg, wsem.at[0])
+    load_l = pltpu.make_async_copy(lin_ref, wl, wsem.at[1])
+    load_g.start()
+    load_l.start()
+    greet_all(z, y, core, x, True)
+
+    def plane_copy(i):
+        return pltpu.make_async_remote_copy(
+            src_ref=blocks_ref.at[i], dst_ref=xb.at[0, i], send_sem=send0.at[i],
+            recv_sem=recv.at[0, i], device_id=plane_place(z, y, core, ORDER[i], 1),
+            device_id_type=MESH,
+        )
+
+    def line_copy(src, group, i, sem, to):
+        return pltpu.make_async_remote_copy(
+            src_ref=src, dst_ref=xb.at[group, i], send_sem=sem.at[i],
+            recv_sem=recv.at[group, i], device_id={"tp": to}, device_id_type=MESH,
+        )
+
+    def own(i):
+        return blocks_ref.at[i] if i == 0 else xb.at[0, i]
+
+    for i in range(1, SLOTS):
+        plane_copy(i).start()
+    xb[0, 0] = blocks_ref[0]
+    for i in range(SLOTS):
+        if i:
+            plane_copy(i).wait_recv()
+        line_copy(own(i), 1, i, send1, right).start()
+        line_copy(own(i), 2, i, send2, left).start()
+    load_g.wait()
+    load_l.wait()
+    r = lax.broadcasted_iota(jnp.int32, (192, 192), 0)
+    c = lax.broadcasted_iota(jnp.int32, (192, 192), 1)
+    within = lax.rem(r, 96)
+    source = (within // CAP) * (2 * CAP) + (r // 96) * CAP + lax.rem(within, CAP)
+    perm = (c == source).astype(f32).astype(bf16)
+
+    def compute(group, part):
+        for s in range(2):
+            for q in range(4):
+                cols = pl.ds(q * 512, 512)
+                raw = xb[group, pl.ds(part * 16 + s * 8, 8), :, cols].reshape(192, 512)
+                fixed = mm(perm, raw).astype(bf16)
+                rows_buf[pl.ds(s * 96, 96), cols] = fixed[:96]
+                rows_buf[pl.ds(s * 96, 96), pl.ds(HALF + q * 512, 512)] = fixed[96:]
+        gate = mm(rows_buf[...], wg[...])
+        lin = mm(rows_buf[...], wl[...])
+        gate = jnp.minimum(gate, 7.0)
+        act = gate * jax.nn.sigmoid(1.702 * gate) * (jnp.clip(lin, -7.0, 7.0) + 1.0)
+        act_buf[group, pl.ds(part * 192, 192), :] = act.astype(bf16)
+
+    def hid_copy(group, to):
+        return pltpu.make_async_remote_copy(
+            src_ref=act_buf.at[group], dst_ref=hid_ref.at[x], send_sem=hsend.at[group],
+            recv_sem=hrecv.at[x], device_id={"tp": to}, device_id_type=MESH,
+        )
+
+    def relay(part):
+        def one(j, carry):
+            a = part * 16 + 2 * j
+            b = a + 1
+            line_copy(xb.at[0, 0], 1, a, send1, right).wait_recv()
+            line_copy(xb.at[1, a], 3, a, send3, right).start()
+            line_copy(xb.at[0, 0], 2, b, send2, left).wait_recv()
+            line_copy(xb.at[2, b], 3, b, send3, left).start()
+            line_copy(xb.at[0, 0], 1, b, send1, right).wait_recv()
+            line_copy(xb.at[0, 0], 2, a, send2, left).wait_recv()
+            return carry
+
+        lax.fori_loop(0, 8, one, 0)
+
+    def far_wait(part):
+        def one(j, carry):
+            line_copy(xb.at[0, 0], 3, part * 16 + j, send3, far).wait_recv()
+            return carry
+
+        lax.fori_loop(0, 16, one, 0)
+
+    def turn(t, carry):
+        @pl.when(jnp.logical_or(t == 2, t == 4))
+        def _():
+            relay((t - 2) // 2)
+
+        @pl.when(t >= 6)
+        def _():
+            far_wait(t - 6)
+
+        middle = jnp.logical_and(t >= 2, t < 6)
+        group = jnp.where(t < 2, 0, jnp.where(middle, 1 + lax.rem(t, 2), 3))
+        part = jnp.where(t < 2, t, jnp.where(middle, (t - 2) // 2, t - 6))
+        compute(group, part)
+
+        @pl.when(t == 4)
+        def _():
+            hid_copy(1, left).start()
+
+        @pl.when(t == 5)
+        def _():
+            hid_copy(2, right).start()
+
+        return carry
+
+    lax.fori_loop(0, 8, turn, 0)
+    hid_copy(3, far).start()
+    hid_ref[x] = act_buf[0]
+    for group, to in ((1, left), (2, right), (3, far)):
+        hid_copy(group, to).wait_send()
+        pltpu.make_async_remote_copy(
+            src_ref=act_buf.at[group], dst_ref=hid_ref.at[to], send_sem=hsend.at[group],
+            recv_sem=hrecv.at[to], device_id={"tp": to}, device_id_type=MESH,
+        ).wait_recv()
+    for i in range(SLOTS):
+        if i:
+            plane_copy(i).wait_send()
+        line_copy(own(i), 1, i, send1, right).wait_send()
+        line_copy(own(i), 2, i, send2, left).wait_send()
+        line_copy(xb.at[1, i], 3, i, send3, right).wait_send()
+
+
+def dispatch(blocks, gate_w, lin_w):
+    width = gate_w.shape[0]
+    dma = pltpu.SemaphoreType.DMA
+    return pl.pallas_call(
+        dispatch_kernel,
+        in_specs=[
+            pl.BlockSpec(memory_space=pltpu.VMEM),
+            pl.BlockSpec(memory_space=pl.ANY),
+            pl.BlockSpec(memory_space=pl.ANY),
+        ],
+        out_specs=pl.BlockSpec(memory_space=pltpu.VMEM),
+        out_shape=jax.ShapeDtypeStruct((4, ROWS, FFD), bf16),
+        scratch_shapes=[
+            pltpu.VMEM((4, SLOTS, 2 * CAP, HALF), bf16),
+            pltpu.VMEM((width, FFD), bf16),
+            pltpu.VMEM((width, FFD), bf16),
+            pltpu.VMEM((192, width), bf16),
+            pltpu.VMEM((4, ROWS, FFD), bf16),
+            dma((2,)), dma((SLOTS,)), dma((SLOTS,)), dma((SLOTS,)), dma((SLOTS,)),
+            dma((4, SLOTS)), dma((4,)), dma((4,)),
+        ],
+        compiler_params=pltpu.CompilerParams(
+            collective_id=1, has_side_effects=True, vmem_limit_bytes=56 * 1024 * 1024
+        ),
+        name="dispatch",
+    )(blocks, gate_w, lin_w)
+
+
+TILE = 512
+
+
+def return_kernel(
+    hid_ref, down_ref, index_ref, weight_ref, stream_ref, out_ref,
+    wd, ready, back, pair_buf, wsem, sends, recvs,
+):
+    z, y, core = (lax.axis_index(a) for a in SP)
+    x = lax.axis_index("tp")
+    steps = HALF // TILE
+
+    def load(j, h):
+        cols = pl.ds(h * HALF + j * TILE, TILE)
+        return pltpu.make_async_copy(down_ref.at[:, cols], wd.at[j, h], wsem.at[j, h])
+
+    for j in range(steps):
+        for h in range(2):
+            load(j, h).start()
+    greet_all(z, y, core, x, False)
+    r = lax.broadcasted_iota(jnp.int32, (192, 192), 0)
+    c = lax.broadcasted_iota(jnp.int32, (192, 192), 1)
+    within = lax.rem(r, 2 * CAP)
+    source = (within // CAP) * 96 + (r // (2 * CAP)) * CAP + lax.rem(within, CAP)
+    perm = (c == source).astype(f32).astype(bf16)
+
+    def send(i, j):
+        return pltpu.make_async_remote_copy(
+            src_ref=ready.at[j, i], dst_ref=back.at[j, i], send_sem=sends.at[j, i],
+            recv_sem=recvs.at[j, i], device_id=plane_place(z, y, core, ORDER[i], -1),
+            device_id_type=MESH,
+        )
+
+    for j in range(steps):
+        for h in range(2):
+            load(j, h).wait()
+            total = mm(hid_ref[0], wd[j, h, pl.ds(0, FFD), :])
+            for k in range(1, 4):
+                total = total + mm(hid_ref[k], wd[j, h, pl.ds(k * FFD, FFD), :])
+            pair_buf[h] = total.astype(bf16)
+        for q in range(4):
+            rows = pl.ds(q * 96, 96)
+            both = jnp.concatenate([pair_buf[0, rows, :], pair_buf[1, rows, :]], axis=0)
+            mixed = mm(perm, both).astype(bf16).reshape(8, 2 * CAP, TILE)
+            ready[j, pl.ds(q * 8, 8)] = mixed
+            for i in range(q * 8, q * 8 + 8):
+                if i:
+                    send(i, j).start()
+        back[j, 0] = ready[j, 0]
+    slots = lax.broadcasted_iota(jnp.int32, (512, SLOTS * 2 * CAP), 1)
+    hot = (slots == index_ref[...]).astype(f32).astype(bf16)
+    for j in range(steps):
+        for i in range(1, SLOTS):
+            send(i, j).wait_recv()
+        arrived = back[j].reshape(SLOTS * 2 * CAP, TILE)
+        for h in range(2):
+            cols = pl.ds(h * HALF + j * TILE, TILE)
+            picked = mm(hot[h * 256 : (h + 1) * 256], arrived)
+            total = stream_ref[:, cols].astype(f32)
+            total = total + picked[:128] * weight_ref[:, 0:1] + picked[128:] * weight_ref[:, 1:2]
+            out_ref[:, cols] = total.astype(bf16)
+    for j in range(steps):
+        for i in range(1, SLOTS):
+            send(i, j).wait_send()
+
+
+def bring_back(hid, down, index, weight, stream):
+    dma = pltpu.SemaphoreType.DMA
+    steps = HALF // TILE
+    vmem = pl.BlockSpec(memory_space=pltpu.VMEM)
+    return pl.pallas_call(
+        return_kernel,
+        in_specs=[vmem, pl.BlockSpec(memory_space=pl.ANY), vmem, vmem, vmem],
+        out_specs=vmem,
+        out_shape=jax.ShapeDtypeStruct(stream.shape, bf16),
+        scratch_shapes=[
+            pltpu.VMEM((steps, 2, 4 * FFD, TILE), bf16),
+            pltpu.VMEM((steps, SLOTS, 2 * CAP, TILE), bf16),
+            pltpu.VMEM((steps, SLOTS, 2 * CAP, TILE), bf16),
+            pltpu.VMEM((2, ROWS, TILE), bf16),
+            dma((steps, 2)), dma((steps, SLOTS)), dma((steps, SLOTS)),
+        ],
+        compiler_params=pltpu.CompilerParams(
+            collective_id=2, has_side_effects=True, vmem_limit_bytes=56 * 1024 * 1024
+        ),
+        name="bring_back",
+    )(hid, down, index, weight, stream)
+
+
+def slot_table(selected):
+    z, y, core = (lax.axis_index(a) for a in SP)
+    count = selected.shape[0]
+    flat = selected.reshape(-1)
+    member = (flat[:, None] == jnp.arange(SLOTS, dtype=jnp.int32)[None, :]).astype(jnp.int32)
+    rank = jnp.sum(jnp.cumsum(member, axis=0) * member, axis=1) - 1
+    away_z = (flat // 8 - z) % 4
+    away_y = (flat // 2 % 4 - y) % 4
+    away = (away_z * 4 + away_y) * 2 + (flat - core) % 2
+    slot = jnp.zeros_like(flat)
+    for i, (dz, dy, dc) in enumerate(ORDER):
+        slot = slot + jnp.where(away == (dz * 4 + dy) * 2 + dc, i, 0)
+    first = (slot * (2 * CAP) + rank).reshape(count, TOPK).T
+    return jnp.stack([first, first + CAP])
+
+
+def expert_layer(stream, normed, selected, route_weight, gate_w, lin_w, down_full):
+    table = slot_table(selected)
+    rows = normed.shape[0]
+    slots = jnp.arange(SLOTS * 2 * CAP, dtype=jnp.int32)[:, None, None]
+    hot = jnp.sum(
+        (slots[..., None] == table.transpose(0, 2, 1)[None]).astype(bf16), axis=-1
+    ).reshape(SLOTS * 2 * CAP, 2 * rows)
+    stacked = jnp.concatenate([normed[:, :HALF], normed[:, HALF:]], axis=0)
+    blocks = jnp.dot(hot, stacked, preferred_element_type=f32).astype(bf16)
+    hid = dispatch(blocks.reshape(SLOTS, 2 * CAP, HALF), gate_w, lin_w)
+    return bring_back(hid, down_full, table.reshape(-1, 1), route_weight, stream)
+
+
 def per_device(
     queries,
     keys,
@@ -395,7 +705,7 @@
     linear_up_weight,
     down_weight,
 ):
-    tok_rows, width_dev = queries.shape
+    down_full = lax.all_gather(down_weight[0], "tp", axis=0, tiled=True)
     head_mix = head_mixing(
         queries,
         keys,
@@ -407,7 +717,6 @@
         head_decay_rate,
         head_norm_gain,
     )
-    local_rows = residual.shape[0]
     mix_sum = summed_on_arrival(
         jnp.dot(head_mix, output_weight, preferred_element_type=jnp.float32).astype(jnp.bfloat16),
         "tp",
@@ -422,59 +731,9 @@
     ).astype(jnp.bfloat16)
     route_exp = jnp.exp(router_chosen_scores)
     route_weight = route_exp / jnp.sum(route_exp, axis=-1, keepdims=True)
-    sp_count = lax.axis_size(SP)
-    tp_count = lax.axis_size("tp")
-    exp_dev = gate_up_weight.shape[0]
-    experts = exp_dev * sp_count
-    capacity = 3 * TOPK * tok_rows // (2 * tp_count * experts)
-    model_width = normed.shape[1]
-    flat_experts = selected_experts.reshape(-1)
-    member = (flat_experts[:, None] == jnp.arange(experts, dtype=jnp.int32)[None, :]).astype(
-        jnp.int32
+    return expert_layer(
+        stream, normed, selected_experts, route_weight, gate_up_weight[0], linear_up_weight[0], down_full
     )
-    slot_rank = jnp.sum(jnp.cumsum(member, axis=0) * member, axis=1) - 1
-    slot_index = flat_experts * capacity + slot_rank
-    slot_hot = (
-        slot_index[:, None] == jnp.arange(experts * capacity, dtype=jnp.int32)[None, :]
-    ).astype(jnp.bfloat16)
-    token_hot = jnp.sum(slot_hot.reshape(local_rows, TOPK, experts * capacity), axis=1)
-    outgoing = jnp.einsum(
-        "rs,rd->sd", token_hot, normed, preferred_element_type=jnp.float32
-    ).astype(jnp.bfloat16)
-    grouped = outgoing.reshape(sp_count, exp_dev, capacity, model_width)
-    copies = jnp.broadcast_to(
-        grouped[:, None], (sp_count, tp_count, exp_dev, capacity, model_width)
-    )
-    copies = copies.reshape(sp_count * tp_count, exp_dev, capacity, model_width)
-    arrived = lax.all_to_all(copies, SP_TP, split_axis=0, concat_axis=0, tiled=True)
-    gate_pre = jnp.einsum(
-        "secd,edf->secf", arrived, gate_up_weight, preferred_element_type=jnp.float32
-    )
-    linear_pre = jnp.einsum(
-        "secd,edf->secf", arrived, linear_up_weight, preferred_element_type=jnp.float32
-    )
-    clipped = jnp.minimum(gate_pre, 7.0)
-    hidden_act = (
-        clipped * jax.nn.sigmoid(1.702 * clipped) * (jnp.clip(linear_pre, -7.0, 7.0) + 1.0)
-    ).astype(jnp.bfloat16)
-    partial_value = jnp.einsum(
-        "secf,efd->secd", hidden_act, down_weight, preferred_element_type=jnp.float32
-    )
-    summed = lax.psum_scatter(
-        partial_value.reshape(sp_count, tp_count, exp_dev, capacity, model_width).astype(
-            jnp.bfloat16
-        ),
-        "tp",
-        scatter_dimension=1,
-        tiled=True,
-    )
-    returned = lax.all_to_all(summed, SP, split_axis=0, concat_axis=0, tiled=True)
-    returned = returned.reshape(experts * capacity, model_width)
-    picked = jnp.dot(slot_hot, returned, preferred_element_type=jnp.float32).reshape(
-        local_rows, TOPK, model_width
-    )
-    combined = jnp.sum(picked * route_weight[:, :, None], axis=1)
-    return (stream_wide + combined).astype(jnp.bfloat16)
 
 
 def solution(mesh):

time: 629 us -> 362 us (0.58); the launches traced: 620 us -> 360 us
  blocking collectives: 196 us -> 0 us
  Pallas kernels: 51.5 us -> 226 us
  waiting for transfers between devices: 210 us -> 91.3 us
  local copies, waits for them, and re-layouts: 74.8 us -> 10.6 us
  matrix products: 52.9 us -> 6.94 us
  starting transfers between devices: 12.5 us -> 5.26 us
    all_to_all x1 -> x0, blocking collectives: 196 us -> none  [per_device(): lax.all_to_all(copies, SP_TP, split_axis=0, concat_axis=0, tiled=True)]
    pallas_call x0 -> x2, Pallas kernels: none -> 174 us  [the longest x1 126 us: dispatch(): pl.pallas_call(dispatch_kernel, in_specs=[pl.BlockSpec(memory_space=pltpu...]
    reduce_scatter x1 -> x0, waiting for transfers between devices: 110 us -> none  [per_device(): lax.psum_scatter(partial_value.reshape(sp_count, tp_count, exp_dev, capac...]
    all_to_all x1 -> x0, waiting for transfers between devices: 53.9 us -> none  [per_device(): lax.all_to_all(summed, SP, split_axis=0, concat_axis=0, tiled=True)]
    dot_general x4 -> x1, matrix products: 48.5 us -> 2.66 us  [expert_layer(): blocks = jnp.dot(hot, stacked, preferred_element_type=f32).astype(bf16)]
    all_to_all x1, waiting for transfers between devices: 46.3 us -> 90.6 us  [summed_on_arrival(): lax.all_to_all(parts, axis, split_axis=0, concat_axis=0, tiled=True)]
    convert_element_type x2 -> x0, local copies, waits for them, and re-layouts: 33.7 us -> none  [per_device(): partial_value.reshape(sp_count, tp_count, exp_dev, capacity, model_width)]
    unnamed x47 -> x38, local copies, waits for them, and re-layouts: 19.4 us -> 8.66 us
  transfers between devices with their start and end apart: 3 -> 2, of which waited for: 3 -> 1; matrix products, arithmetic and copies ran while one was open for 0% -> 4% of each run, Pallas kernels for 0% -> 49%
where the time goes in v2:
time: 362 us; the launch traced here: 360 us
  Pallas kernels  226 us (62%)
  waiting for transfers between devices  91.3 us (25%)
  between operations  13.7 us (4%)
  local copies, waits for them, and re-layouts  10.6 us (3%)
  matrix products  6.94 us (2%)
  other arithmetic  5.86 us (2%)
  starting transfers between devices  5.26 us (1%)
    pallas_call x1, Pallas kernels, dispatch(): pl.pallas_call(dispatch_kernel, in_specs=[pl.BlockSpec(memory_space=pltpu...  126 us
    all_to_all x1, waiting for transfers between devices, summed_on_arrival(): lax.all_to_all(parts, axis, split_axis=0, concat_axis=0, tiled=True)  90.6 us
    pallas_call x1, Pallas kernels, bring_back(): pl.pallas_call(return_kernel, in_specs=[vmem, pl.BlockSpec(memory_space=p...  48.9 us
    pallas_call x1, Pallas kernels, exchange(): pl.pallas_call(exchange_kernel, in_specs=[pl.BlockSpec(memory_space=pltpu...  36.6 us
    pallas_call x1, Pallas kernels, local_pass(): pl.pallas_call(local_kernel, grid=(heads,), in_specs=[columns, columns, c...  12.1 us
    unnamed x38, local copies, waits for them, and re-layouts  8.66 us
  transfers between devices with their start and end apart: 2, of which 1 were waited for; matrix products, arithmetic and copies ran while one was open for 4% of the time, Pallas kernels for 49%

profile of v2, /device:TPU:0, one launch (start us, length us, event | category | flops | bytes accessed | tf_op | source)
XLA Modules:
  0.0 360.0 jit_solution(16451345751576396177)
XLA Ops:
  6.5 0.0 copy-start.15
  6.5 0.0 copy-start.11
  6.5 0.0 copy-start.10
  6.5 0.0 copy-start.12
  6.5 0.0 copy-start.2
  6.5 0.0 copy-start.3
  6.6 0.0 all-gather.3.cloned.1.call-start
  6.6 0.7 all-gather.3.cloned.1.call-update
  7.3 0.0 copy-done.15
  7.3 0.0 copy-start.7
  7.3 0.0 copy-done.11
  7.3 0.0 copy-done.10
  7.3 0.1 fusion.13
  7.5 0.0 copy-done.12
  7.5 0.1 copy-done.2
  7.6 0.2 copy-done.3
  7.8 0.0 copy-start.4
  7.8 1.0 copy-done.4
  8.8 12.1 %local_pass.1 = (f32[512,512]{1,0:T(8,128)S(1)}, bf16[4,512,256]{2,1,0:T(8,128)(2,1)S(1)}, bf16[4,8,128,256]{3,2,1,0:T(8,128)(2,1)}, bf16[4,2,128,256]{3,2,1,0:T(8,128)(2,1)S(1)}) custom-call(bf16[512,512]{1,0:T(8,128)(2,1)S(1)} %copy-done.2, bf16[512,512]{1,0:T(8,128)(2,1)S(1)} %copy-done.3, bf16[512,512]{1,0:T(8,128)(2,1)S(1)} %copy-done.4, ...), custom_call_target="tpu_custom_call" | custom-call | tf_op jit(solution)/shard_map/local_pass/pallas_call | solution.py:118
  20.9 0.0 copy-start.5
  20.9 0.8 copy-done.5
  21.7 36.6 %exchange.1 = bf16[8,128,128]{2,1,0:T(8,128)(2,1)} custom-call(bf16[8,128,256]{2,1,0:T(8,128)(2,1)} %bitcast.43), custom_call_target="tpu_custom_call" | custom-call | tf_op jit(solution)/shard_map/exchange/pallas_call | solution.py:283
  58.3 0.0 copy-done.7
  58.3 0.0 copy-start
  58.4 1.6 copy-done
  60.0 0.0 copy-start.1
  60.0 0.9 copy-done.1
  60.9 0.0 copy-start.6
  60.9 1.0 copy-done.6
  61.9 3.3 finish_pass.1
  65.3 0.0 copy-done.17
  65.3 4.3 %convolution_convert_fusion = bf16[512,4096]{1,0:T(8,128)(2,1)} fusion(bf16[512,512]{1,0:T(8,128)(2,1)S(1)} %finish_pass.1, bf16[512,4096]{1,0:T(8,128)(2,1)S(1)} %copy-done.17), kind=kOutput, calls=%fused_computation.1 | convolution fusion | flops 2149580800 | bytes 8912896 | tf_op jit(solution)/shard_map/dot_general | solution.py:721
  69.6 0.0 copy-start.14
  69.6 5.2 %all-to-all-start = ((bf16[4,128,4096]{2,1,0:T(8,128)(2,1)}), bf16[4,128,4096]{2,1,0:T(8,128)(2,1)}, u32[]{:S(2)}, u32[]{:S(2)}) async-start(bf16[4,128,4096]{2,1,0:T(8,128)(2,1)} %bitcast.47), calls=%async_computation | async-start | bytes 8388608 | tf_op jit(solution)/shard_map/all_to_all | solution.py:375
  74.8 0.0 copy-done.14
  74.8 0.1 copy.119
  74.9 0.1 eq.271
  75.1 0.1 eq.267
  75.2 0.0 copy-done.13
  75.3 0.6 reduce-window.6
  75.8 0.2 slice_reduce_fusion
  76.1 0.1 fusion.9
  76.2 0.1 sub.45
  76.3 0.1 copy.122
  76.4 0.1 fusion.54
  76.5 0.2 fusion.7
  76.7 0.2 copy.123
  76.9 0.9 copy.127.index_ref
  77.7 0.0 copy-done.16
  77.7 0.1 copy.126
  77.8 0.7 broadcast_divide_fusion.weight_ref
  78.6 90.6 %all-to-all-done = bf16[4,128,4096]{2,1,0:T(8,128)(2,1)} async-done(((bf16[4,128,4096]{2,1,0:T(8,128)(2,1)}), bf16[4,128,4096]{2,1,0:T(8,128)(2,1)}, u32[]{:S(2)}, u32[]{:S(2)}) %all-to-all-start) | async-done | bytes 4194336 | tf_op jit(solution)/shard_map/all_to_all | solution.py:375
  169.1 3.2 convert_reduce_fusion
  172.4 0.0 copy-done.9
  172.4 0.4 fusion
  172.8 0.0 copy-start.8
  172.9 0.3 fusion.2
  173.2 0.1 fusion.58
  173.3 0.5 copy-done.8
  173.8 2.7 convolution_convert_fusion.1
  176.5 125.5 %dispatch.1.hid_ref = bf16[4,384,384]{2,1,0:T(8,128)(2,1)} custom-call(bf16[32,24,2048]{2,1,0:T(8,128)(2,1)} %bitcast.45, bf16[4096,384]{1,0:T(8,128)(2,1)} %bitcast.48, bf16[4096,384]{1,0:T(8,128)(2,1)} %bitcast.49), custom_call_target="tpu_custom_call" | custom-call | tf_op jit(solution)/shard_map/dispatch/pallas_call | solution.py:547
  302.0 0.0 all-gather.3.cloned.1.call-done
  302.0 48.9 %bring_back.1 = bf16[128,4096]{1,0:T(8,128)(2,1)} custom-call(bf16[4,384,384]{2,1,0:T(8,128)(2,1)} %dispatch.1.hid_ref, bf16[1536,4096]{1,0:T(8,128)(2,1)} %bitcast.46, s32[512,1]{1,0:T(8,128)} %copy.127.index_ref, f32[128,2]{1,0:T(8,128)} %broadcast_divide_fusion.weight_ref, bf16[128,4096]{1,0:T(8,128)(2,1)} %copy-done.8), custom_call_target="tpu_custom_call" | custom-call | tf_op jit(solution)/shard_map/bring_back/pallas_call | solution.py:641
  350.9 2.3 copy.131
  (18 shorter events, 0.2 us)
Async XLA Ops:
  6.5 0.8 copy-start.15
  6.5 0.8 copy-start.11
  6.5 0.8 copy-start.10
  6.5 0.9 copy-start.12
  6.5 1.1 copy-start.2
  6.5 1.3 copy-start.3
  6.6 295.4 %all-gather.3.cloned.1.call-start = ((), (), s32[]{:S(2)}) async-start(), calls=%async_computation.1 | async-start | bytes 15728640 | tf_op jit(solution)/shard_map/all_gather | solution.py:708
  7.3 51.0 %copy-start.7 = (bf16[128]{0:T(256)(128)(2,1)S(1)}, bf16[128]{0:T(256)(128)(2,1)}, u32[]{:S(2)}) copy-start(bf16[128]{0:T(256)(128)(2,1)} %param.25) | copy-start | bytes 772
  7.8 1.0 copy-start.4
  20.9 0.8 copy-start.5
  58.3 1.6 copy-start
  60.0 0.9 copy-start.1
  60.9 1.0 copy-start.6
  61.9 3.3 copy-start.17
  69.6 5.2 %copy-start.14 = (s32[128,2]{0,1:T(2,128)S(1)}, s32[128,2]{0,1:T(2,128)}, u32[]{:S(2)}) copy-start(s32[128,2]{0,1:T(2,128)} %param.29) | copy-start | bytes 3076
  69.6 5.7 %copy-start.13 = (bf16[4096]{0:T(1024)(128)(2,1)S(1)}, bf16[4096]{0:T(1024)(128)(2,1)}, u32[]{:S(2)}) copy-start(bf16[4096]{0:T(1024)(128)(2,1)} %param.28) | copy-start | bytes 24580
  69.6 8.1 %copy-start.16 = (f32[128,2]{0,1:T(2,128)S(1)}, f32[128,2]{0,1:T(2,128)}, u32[]{:S(2)}) copy-start(f32[128,2]{0,1:T(2,128)} %param.30) | copy-start | bytes 3076
  69.6 99.6 %all-to-all-start = ((bf16[4,128,4096]{2,1,0:T(8,128)(2,1)}), bf16[4,128,4096]{2,1,0:T(8,128)(2,1)}, u32[]{:S(2)}, u32[]{:S(2)}) async-start(bf16[4,128,4096]{2,1,0:T(8,128)(2,1)} %bitcast.47), calls=%async_computation | async-start | bytes 8388608 | tf_op jit(solution)/shard_map/all_to_all | solution.py:375
  78.6 93.8 %copy-start.9 = (bf16[128,4096]{1,0:T(8,128)(2,1)S(1)}, bf16[128,4096]{1,0:T(8,128)(2,1)}, u32[]{:S(2)}) copy-start(bf16[128,4096]{1,0:T(8,128)(2,1)} %param.27) | copy-start | bytes 3145732
  172.8 1.0 copy-start.8
Sparse Core Ops, SparseCore 0:
  9.0 165.9 all-gather.2

commit v3 on v1

--- a/solution.py
+++ b/solution.py
@@ -132,14 +132,24 @@
             jax.ShapeDtypeStruct((heads, 2, n, 2 * n), bf16),
         ],
         compiler_params=ARB,
+        cost_estimate=pl.CostEstimate(flops=4 * 10**9, bytes_accessed=8 * 10**6, transcendentals=0),
         name="local_pass",
     )(queries, keys, values, log_decay, beta)
 
 
-def exchange_kernel(comp_ref, out_ref, got, pre, chunk, start, ready, send1, recv1, send2, recv2):
+def exchange_kernel(
+    comp_ref, down_ref, out_ref, quarter_ref,
+    got, pre, chunk, start, ready, held_w, send1, recv1, send2, recv2, wsem, wsend, wrecv,
+):
     n = BLOCK
     z, y, core = (lax.axis_index(a) for a in SP)
+    x = lax.axis_index("tp")
     me = (z * 4 + y) * 2 + core
+    depth, part = down_ref.shape[0], down_ref.shape[1] // 4
+    take = pltpu.make_async_copy(
+        down_ref.at[:, pl.ds(pl.multiple_of(x * part, part), part)], held_w, wsem.at[0]
+    )
+    take.start()
     is_owner = jnp.logical_and(core == 1, y % 2 == z % 2)
     way = y // 2
     mine = z * 2 + way
@@ -155,7 +165,11 @@
         return carry
 
     lax.fori_loop(1, 32, greet, 0)
-    pl.semaphore_wait(barrier, 31)
+    for dx in range(1, 4):
+        pl.semaphore_signal(
+            barrier, inc=1, device_id={"tp": lax.rem(x + dx, 4)}, device_id_type=MESH
+        )
+    pl.semaphore_wait(barrier, 34)
 
     def owner_of(c):
         oz = c // 2
@@ -181,6 +195,26 @@
         @pl.when(me == own)
         def _():
             got[me] = comp_ref[c]
+
+    def mine_rows(at):
+        return quarter_ref.at[pl.ds(pl.multiple_of(at * depth, depth), depth), :]
+
+    def weight_copy(dx):
+        to = lax.rem(x + dx, 4)
+        return pltpu.make_async_remote_copy(
+            src_ref=down_ref.at[:, pl.ds(pl.multiple_of(to * part, part), part)],
+            dst_ref=mine_rows(x),
+            send_sem=wsend.at[dx],
+            recv_sem=wrecv.at[dx],
+            device_id={"tp": to},
+            device_id_type=MESH,
+        )
+
+    for dx in range(1, 4):
+        weight_copy(dx).start()
+    take.wait()
+    put = pltpu.make_async_copy(held_w, mine_rows(x), wsem.at[1])
+    put.start()
 
     def arrival(s):
         return pltpu.make_async_remote_copy(
@@ -277,28 +311,49 @@
                 device_id_type=MESH,
             ).wait_recv()
 
-
-def exchange(comp):
+    put.wait()
+    for dx in range(1, 4):
+        weight_copy(dx).wait_send()
+        pltpu.make_async_remote_copy(
+            src_ref=down_ref.at[:, pl.ds(0, part)],
+            dst_ref=mine_rows(lax.rem(x + 4 - dx, 4)),
+            send_sem=wsend.at[dx],
+            recv_sem=wrecv.at[dx],
+            device_id={"tp": lax.rem(x + 4 - dx, 4)},
+            device_id_type=MESH,
+        ).wait_recv()
+
+
+def exchange(comp, down):
     n = BLOCK
+    depth, part = down.shape[0], down.shape[1] // 4
     return pl.pallas_call(
         exchange_kernel,
-        in_specs=[pl.BlockSpec(memory_space=pltpu.VMEM)],
-        out_specs=pl.BlockSpec(memory_space=pltpu.VMEM),
-        out_shape=jax.ShapeDtypeStruct((8, n, n), bf16),
+        in_specs=[pl.BlockSpec(memory_space=pltpu.VMEM), pl.BlockSpec(memory_space=pl.ANY)],
+        out_specs=[pl.BlockSpec(memory_space=pltpu.VMEM), pl.BlockSpec(memory_space=pl.ANY)],
+        out_shape=[
+            jax.ShapeDtypeStruct((8, n, n), bf16),
+            jax.ShapeDtypeStruct((4 * depth, part), bf16),
+        ],
         scratch_shapes=[
             pltpu.VMEM((32, n, 2 * n), bf16),
             pltpu.VMEM((32, n, 2 * n), bf16),
             pltpu.VMEM((4, n, 2 * n), f32),
             pltpu.VMEM((4, n, n), bf16),
             pltpu.VMEM((32, n, n), bf16),
+            pltpu.VMEM((depth, part), bf16),
             pltpu.SemaphoreType.DMA((8,)),
             pltpu.SemaphoreType.DMA((32,)),
             pltpu.SemaphoreType.DMA((32,)),
             pltpu.SemaphoreType.DMA((8,)),
+            pltpu.SemaphoreType.DMA((2,)),
+            pltpu.SemaphoreType.DMA((4,)),
+            pltpu.SemaphoreType.DMA((4,)),
         ],
         compiler_params=pltpu.CompilerParams(collective_id=0, has_side_effects=True),
+        cost_estimate=pl.CostEstimate(flops=9 * 10**9, bytes_accessed=8 * 10**6, transcendentals=0),
         name="exchange",
-    )(comp)
+    )(comp, down)
 
 
 def finish_kernel(out_ref, qeff_ref, blk_ref, sin_ref, gate_ref, gain_ref, mix_ref):
@@ -345,7 +400,61 @@
     )(out_local, qeff, blk, entering, gates, gain)
 
 
-def head_mixing(queries, keys, values, gates, decay_logits, write_logits, extra, rate, gain):
+def swap_kernel(mix_ref, out_ref, own_sem, send, recv):
+    x = lax.axis_index("tp")
+    rows, part = mix_ref.shape[0] // 4, mix_ref.shape[1]
+    barrier = pltpu.get_barrier_semaphore()
+    for dx in range(1, 4):
+        pl.semaphore_signal(
+            barrier, inc=1, device_id={"tp": lax.rem(x + dx, 4)}, device_id_type=MESH
+        )
+    pl.semaphore_wait(barrier, 3)
+
+    def rows_of(at):
+        return mix_ref.at[pl.ds(pl.multiple_of(at * rows, rows), rows), :]
+
+    def place_of(half, at):
+        return out_ref.at[
+            pl.ds(half * rows, rows), pl.ds(pl.multiple_of(at * part, part), part)
+        ]
+
+    def copy(half, dx, back):
+        to = lax.rem(x + (4 - dx if back else dx), 4)
+        return pltpu.make_async_remote_copy(
+            src_ref=rows_of(lax.rem(to + 2 * half, 4)), dst_ref=place_of(half, to if back else x),
+            send_sem=send.at[half, dx], recv_sem=recv.at[half, dx], device_id={"tp": to},
+            device_id_type=MESH,
+        )
+
+    for dx in (2, 1, 3):
+        for half in range(2):
+            copy(half, dx, False).start()
+    for half in range(2):
+        own = pltpu.make_async_copy(
+            rows_of(lax.rem(x + 2 * half, 4)), place_of(half, x), own_sem.at[half]
+        )
+        own.start()
+        own.wait()
+    for dx in (1, 3, 2):
+        for half in range(2):
+            copy(half, dx, False).wait_send()
+            copy(half, dx, True).wait_recv()
+
+
+def swap(mix):
+    dma = pltpu.SemaphoreType.DMA
+    return pl.pallas_call(
+        swap_kernel,
+        in_specs=[pl.BlockSpec(memory_space=pltpu.VMEM)],
+        out_specs=pl.BlockSpec(memory_space=pltpu.VMEM),
+        out_shape=jax.ShapeDtypeStruct((mix.shape[0] // 2, mix.shape[1] * 4), bf16),
+        scratch_shapes=[dma((2,)), dma((2, 4)), dma((2, 4))],
+        compiler_params=pltpu.CompilerParams(collective_id=3, has_side_effects=True),
+        name="swap",
+    )(mix)
+
+
+def head_mixing(queries, keys, values, gates, decay_logits, write_logits, extra, rate, gain, down):
     tok, width = queries.shape
     heads = width // HEAD_DIM
     log_decay = -rate[:, None, :] * jax.nn.softplus(decay_logits) + extra
@@ -358,22 +467,309 @@
     out_local, qeff, blk, comp = local_pass(
         queries, keys, values, per_head(log_decay), per_head(beta), heads
     )
-    entering = exchange(comp.reshape(2 * heads, BLOCK, 2 * BLOCK))
-    return finish_pass(
+    entering, down_quarter = exchange(comp.reshape(2 * heads, BLOCK, 2 * BLOCK), down)
+    mix = finish_pass(
         out_local, qeff, blk, entering.reshape(heads, 2, BLOCK, BLOCK), gates, gain.reshape(1, -1)
     )
-
-
-def in_blocks(shard, dim, count):
-    shape = shard.shape
-    parts = shard.reshape(*shape[:dim], count, shape[dim] // count, *shape[dim + 1 :])
-    return jnp.moveaxis(parts, dim, 0)
-
-
-def summed_on_arrival(shard, axis, dim):
-    parts = in_blocks(shard, dim, lax.axis_size(axis))
-    arrived = lax.all_to_all(parts, axis, split_axis=0, concat_axis=0, tiled=True)
-    return arrived.astype(jnp.float32).sum(axis=0)
+    return swap(mix), down_quarter
+
+
+ORDER = (
+    (0, 0, 0), (2, 2, 1), (0, 0, 1), (2, 2, 0), (0, 1, 0), (2, 3, 1), (0, 1, 1), (2, 3, 0),
+    (1, 0, 0), (2, 1, 1), (1, 0, 1), (2, 1, 0), (0, 3, 0), (3, 2, 1), (0, 3, 1), (3, 2, 0),
+    (3, 0, 0), (1, 2, 1), (3, 0, 1), (1, 2, 0), (1, 1, 0), (2, 0, 1), (1, 1, 1), (2, 0, 0),
+    (3, 3, 0), (0, 2, 1), (3, 3, 1), (0, 2, 0), (1, 3, 0), (3, 1, 1), (1, 3, 1), (3, 1, 0),
+)
+CAP = 12
+TILE = 512
+AHEAD = 8
+SLOTS = len(ORDER)
+HALF = 2048
+FFD = 384
+ROWS = SLOTS * CAP
+
+
+def plane_place(z, y, core, offset, sign):
+    dz, dy, dc = offset
+    return {
+        "sp_0": lax.rem(z + (dz if sign > 0 else 4 - dz), 4),
+        "sp_1": lax.rem(y + (dy if sign > 0 else 4 - dy), 4),
+        "sp_2": lax.rem(core + dc, 2),
+    }
+
+
+def dispatch_kernel(
+    blocks_ref, gate_ref, lin_ref, down_ref, index_ref, weight_ref, stream_ref, out_ref,
+    xb, wg, wl, act_buf, hid_ref, wd, ready, back,
+    wsem, send0, send1, recv, hsend, rsend, hrecv, hfar, sends, recvs,
+):
+    z, y, core = (lax.axis_index(a) for a in SP)
+    x = lax.axis_index("tp")
+    right, left, far = lax.rem(x + 1, 4), lax.rem(x + 3, 4), lax.rem(x + 2, 4)
+    keep = pltpu.make_async_copy(blocks_ref.at[0], xb.at[0, 0], wsem.at[2])
+    keep.start()
+    load_g = pltpu.make_async_copy(gate_ref, wg, wsem.at[0])
+    load_l = pltpu.make_async_copy(lin_ref, wl, wsem.at[1])
+    load_g.start()
+    load_l.start()
+    load_d = pltpu.make_async_copy(down_ref, wd, wsem.at[3])
+    load_d.start()
+    barrier = pltpu.get_barrier_semaphore()
+    for dx in range(4):
+        for offset in ORDER:
+            if dx or offset != ORDER[0]:
+                to = plane_place(z, y, core, offset, 1)
+                to["tp"] = lax.rem(x + dx, 4)
+                pl.semaphore_signal(barrier, inc=1, device_id=to, device_id_type=MESH)
+    pl.semaphore_wait(barrier, 4 * SLOTS - 1)
+
+    def plane_copy(i):
+        return pltpu.make_async_remote_copy(
+            src_ref=blocks_ref.at[i], dst_ref=xb.at[0, i], send_sem=send0.at[i],
+            recv_sem=recv.at[0, i], device_id=plane_place(z, y, core, ORDER[i], 1),
+            device_id_type=MESH,
+        )
+
+    def line_copy(i, to):
+        return pltpu.make_async_remote_copy(
+            src_ref=xb.at[0, i], dst_ref=xb.at[1, i], send_sem=send1.at[i],
+            recv_sem=recv.at[1, i], device_id={"tp": to}, device_id_type=MESH,
+        )
+
+    def arrival(pair, i):
+        return pltpu.make_async_remote_copy(
+            src_ref=blocks_ref.at[0], dst_ref=xb.at[pair, i], send_sem=send0.at[0],
+            recv_sem=recv.at[pair, i], device_id={"tp": right}, device_id_type=MESH,
+        )
+
+    for i in range(1, AHEAD + 1):
+        plane_copy(i).start()
+    keep.wait()
+    r = lax.broadcasted_iota(jnp.int32, (192, 192), 0)
+    c = lax.broadcasted_iota(jnp.int32, (192, 192), 1)
+    within = lax.rem(r, 96)
+    source = (within // CAP) * (2 * CAP) + (r // 96) * CAP + lax.rem(within, CAP)
+    perm = (c == source).astype(f32).astype(bf16)
+    source_2 = (lax.rem(r, 2 * CAP) // CAP) * 96 + (r // (2 * CAP)) * CAP + lax.rem(
+        lax.rem(r, 2 * CAP), CAP
+    )
+    perm_2 = (c == source_2).astype(f32).astype(bf16)
+    parity = lax.rem(x, 2)
+    load_g.wait()
+    load_l.wait()
+    load_d.wait()
+
+    def compute(pair, part):
+        rows = xb[pair, pl.ds(part * 8, 8)].reshape(192, 2 * HALF)
+        gate = jnp.minimum(mm(rows, wg[...]), 7.0)
+        lin = mm(rows, wl[...])
+        act = gate * jax.nn.sigmoid(1.702 * gate) * (jnp.clip(lin, -7.0, 7.0) + 1.0)
+        fixed = mm(perm, act.astype(bf16)).astype(bf16)
+        low = parity if pair == 0 else 1 - parity
+        for half in range(2):
+            piece = fixed[half * 96 : (half + 1) * 96]
+            act_buf[part, low + 2 * half] = piece
+            hid_ref[part, x, low + 2 * half] = piece
+
+    def hid_copy(part, way):
+        return pltpu.make_async_remote_copy(
+            src_ref=act_buf.at[part], dst_ref=hid_ref.at[part, x],
+            send_sem=hsend.at[part, way], recv_sem=hrecv.at[part, x],
+            device_id={"tp": lax.rem(x + way, 4)}, device_id_type=MESH,
+        )
+
+    def hid_arrival(part, piece):
+        return pltpu.make_async_remote_copy(
+            src_ref=act_buf.at[part], dst_ref=hid_ref.at[part, piece],
+            send_sem=hsend.at[part, 1], recv_sem=hrecv.at[part, piece],
+            device_id={"tp": right}, device_id_type=MESH,
+        )
+
+    def hid_relay(part, half, piece, to):
+        here = hid_ref.at[part, piece, pl.ds(2 * half, 2)]
+        return pltpu.make_async_remote_copy(
+            src_ref=here, dst_ref=here, send_sem=rsend.at[part, half],
+            recv_sem=hfar.at[part, half], device_id={"tp": to}, device_id_type=MESH,
+        )
+
+    def relay(part):
+        hid_arrival(part, left).wait_recv()
+        hid_relay(part, 0, left, right).start()
+        hid_arrival(part, right).wait_recv()
+        hid_relay(part, 1, right, left).start()
+
+    def send(i, dx):
+        to = plane_place(z, y, core, ORDER[i], -1)
+        to["tp"] = lax.rem(x + dx, 4)
+        return pltpu.make_async_remote_copy(
+            src_ref=ready.at[dx, i], dst_ref=back.at[x, i], send_sem=sends.at[dx, i],
+            recv_sem=recvs.at[x, i], device_id=to, device_id_type=MESH,
+        )
+
+    def project(part):
+        totals = []
+        for h in range(2):
+            cols = pl.ds(h * TILE, TILE)
+            total = mm(hid_ref[part, 0].reshape(ROWS, FFD), wd[pl.ds(0, FFD), cols])
+            for k in range(1, 4):
+                piece = hid_ref[part, k].reshape(ROWS, FFD)
+                total = total + mm(piece, wd[pl.ds(k * FFD, FFD), cols])
+            totals.append(total.astype(bf16))
+        for group in range(4):
+            rows = slice(group * 96, (group + 1) * 96)
+            both = jnp.concatenate([totals[0][rows], totals[1][rows]], axis=0)
+            mixed = mm(perm_2, both).astype(bf16).reshape(8, 2 * CAP, TILE)
+            ready[lax.rem(group + 4 - x, 4), pl.ds(part * 8, 8)] = mixed
+        for q in range(4):
+
+            @pl.when(part == q)
+            def _():
+                for i in range(8 * q, 8 * q + 8):
+                    for dx in (2, 1, 3, 0):
+                        if i or dx:
+                            send(i, dx).start()
+
+    def turn(part, carry):
+        for p in range(4):
+
+            @pl.when(part == p)
+            def _():
+                for i in range(8 * p, 8 * p + 8):
+                    if i:
+                        if i + AHEAD < SLOTS:
+                            plane_copy(i).wait_send()
+                            plane_copy(i + AHEAD).start()
+                        arrival(0, i).wait_recv()
+                    line_copy(i, left if i % 2 else right).start()
+
+        @pl.when(part > 0)
+        def _():
+            relay(part - 1)
+
+        @pl.when(part < 4)
+        def _():
+            compute(0, part)
+
+            def landed(j, carry):
+                arrival(1, part * 8 + j).wait_recv()
+                return carry
+
+            lax.fori_loop(0, 8, landed, 0)
+            compute(1, part)
+            hid_copy(part, 1).start()
+            hid_copy(part, 3).start()
+
+        @pl.when(part > 0)
+        def _():
+            for half in range(2):
+                hid_relay(part - 1, half, far, right).wait_recv()
+            project(part - 1)
+
+        return carry
+
+    lax.fori_loop(0, 5, turn, 0)
+    back[x, 0] = ready[0, 0]
+    slots = lax.broadcasted_iota(jnp.int32, (512, SLOTS * 2 * CAP), 1)
+    hot = (slots == index_ref[...]).astype(f32).astype(bf16)
+    for dx in (0, 1, 3, 2):
+        piece = lax.rem(x + dx, 4)
+        for i in range(SLOTS):
+            if i or dx:
+                pltpu.make_async_remote_copy(
+                    src_ref=ready.at[0, 0], dst_ref=back.at[piece, i], send_sem=sends.at[0, 0],
+                    recv_sem=recvs.at[piece, i], device_id={"tp": right},
+                    device_id_type=MESH,
+                ).wait_recv()
+        arrived = back[piece].reshape(SLOTS * 2 * CAP, TILE)
+        for h in range(2):
+            cols = pl.ds(pl.multiple_of(piece * (2 * TILE) + h * TILE, TILE), TILE)
+            picked = mm(hot[h * 256 : (h + 1) * 256], arrived)
+            total = stream_ref[:, cols].astype(f32)
+            total = total + picked[:128] * weight_ref[:, 0:1] + picked[128:] * weight_ref[:, 1:2]
+            out_ref[:, cols] = total.astype(bf16)
+
+    def finish(part, carry):
+        for half in range(2):
+            hid_relay(part, half, far, right).wait_send()
+        hid_copy(part, 1).wait_send()
+        hid_copy(part, 3).wait_send()
+        return carry
+
+    lax.fori_loop(0, 4, finish, 0)
+    for i in range(SLOTS):
+        if i + AHEAD >= SLOTS:
+            plane_copy(i).wait_send()
+        line_copy(i, right).wait_send()
+        for dx in range(4):
+            if i or dx:
+                send(i, dx).wait_send()
+
+
+def dispatch(blocks, gate_w, lin_w, down, index, weight, stream):
+    width = gate_w.shape[0]
+    dma = pltpu.SemaphoreType.DMA
+    vmem, far_off = (pl.BlockSpec(memory_space=m) for m in (pltpu.VMEM, pl.ANY))
+    return pl.pallas_call(
+        dispatch_kernel,
+        in_specs=[vmem, far_off, far_off, far_off, vmem, vmem, vmem],
+        out_specs=vmem,
+        out_shape=jax.ShapeDtypeStruct(stream.shape, bf16),
+        scratch_shapes=[
+            pltpu.VMEM((2, SLOTS, 2 * CAP, width), bf16),
+            pltpu.VMEM((width, FFD), bf16),
+            pltpu.VMEM((width, FFD), bf16),
+            pltpu.VMEM((4, 4, 96, FFD), bf16),
+            pltpu.VMEM((4, 4, 4, 96, FFD), bf16),
+            pltpu.VMEM(down.shape, bf16),
+            pltpu.VMEM((4, SLOTS, 2 * CAP, TILE), bf16),
+            pltpu.VMEM((4, SLOTS, 2 * CAP, TILE), bf16),
+            dma((4,)), dma((SLOTS,)), dma((SLOTS,)), dma((2, SLOTS)),
+            dma((4, 4)), dma((4, 2)), dma((4, 4)), dma((4, 2)), dma((4, SLOTS)), dma((4, SLOTS)),
+        ],
+        compiler_params=pltpu.CompilerParams(
+            collective_id=1, has_side_effects=True, vmem_limit_bytes=58 * 1024 * 1024
+        ),
+        name="experts",
+    )(blocks, gate_w, lin_w, down, index, weight, stream)
+
+
+def slot_table(selected):
+    z, y, core = (lax.axis_index(a) for a in SP)
+    count = selected.shape[0]
+    flat = selected.reshape(-1)
+    member = (flat[:, None] == jnp.arange(SLOTS, dtype=jnp.int32)[None, :]).astype(jnp.int32)
+    rank = jnp.sum(jnp.cumsum(member, axis=0) * member, axis=1) - 1
+    away_z = (flat // 8 - z) % 4
+    away_y = (flat // 2 % 4 - y) % 4
+    away = (away_z * 4 + away_y) * 2 + (flat - core) % 2
+    slot = jnp.zeros_like(flat)
+    for i, (dz, dy, dc) in enumerate(ORDER):
+        slot = slot + jnp.where(away == (dz * 4 + dy) * 2 + dc, i, 0)
+    return slot.reshape(count, TOPK), rank.reshape(count, TOPK)
+
+
+def expert_layer(stream, normed, selected, other, route_weight, gate_w, lin_w, down_quarter):
+    rows = selected.shape[0]
+    late = lax.axis_index("tp") // 2
+    slot, rank = slot_table(selected)
+    first = slot * (2 * CAP) + rank
+    table = jnp.stack([first.T, first.T + CAP])
+    slot_2, rank_2 = slot_table(other)
+    source = jnp.concatenate(
+        [first + late * CAP, slot_2 * (2 * CAP) + rank_2 + (1 - late) * CAP], axis=0
+    )
+    slots = jnp.arange(SLOTS * 2 * CAP, dtype=jnp.int32)[:, None]
+    hot = (slots == source[None, :, 0]).astype(bf16) + (slots == source[None, :, 1]).astype(bf16)
+    blocks = jnp.dot(hot, normed, preferred_element_type=f32).astype(bf16)
+    return dispatch(
+        blocks.reshape(SLOTS, 2 * CAP, 2 * HALF),
+        gate_w,
+        lin_w,
+        down_quarter,
+        table.reshape(4 * rows, 1),
+        route_weight,
+        stream,
+    )
 
 
 def per_device(
@@ -395,8 +791,14 @@
     linear_up_weight,
     down_weight,
 ):
-    tok_rows, width_dev = queries.shape
-    head_mix = head_mixing(
+    place = (lax.axis_index("sp_0") * 4 + lax.axis_index("sp_1")) * 2 + lax.axis_index("sp_2")
+    few = output_weight.shape[0] // lax.axis_size(SP)
+    own_rows = lax.dynamic_slice_in_dim(output_weight, place * few, few, axis=0)
+    full_weight = lax.all_gather(own_rows, ("tp",) + SP, axis=0, tiled=True)
+    opposite = [(i, (i + 2) % 4) for i in range(4)]
+    residual_2 = lax.ppermute(residual, "tp", opposite)
+    selected_2 = lax.ppermute(selected_experts, "tp", opposite)
+    head_mix, down_quarter = head_mixing(
         queries,
         keys,
         values,
@@ -406,14 +808,11 @@
         extra_log_decay,
         head_decay_rate,
         head_norm_gain,
-    )
-    local_rows = residual.shape[0]
-    mix_sum = summed_on_arrival(
-        jnp.dot(head_mix, output_weight, preferred_element_type=jnp.float32).astype(jnp.bfloat16),
-        "tp",
-        0,
-    )
-    stream = (residual.astype(jnp.float32) + mix_sum).astype(jnp.bfloat16)
+        down_weight[0],
+    )
+    mix_sum = jnp.dot(head_mix, full_weight, preferred_element_type=jnp.float32)
+    both = jnp.concatenate([residual, residual_2], axis=0)
+    stream = (both.astype(jnp.float32) + mix_sum).astype(jnp.bfloat16)
     stream_wide = stream.astype(jnp.float32)
     normed = (
         stream_wide
@@ -422,59 +821,16 @@
     ).astype(jnp.bfloat16)
     route_exp = jnp.exp(router_chosen_scores)
     route_weight = route_exp / jnp.sum(route_exp, axis=-1, keepdims=True)
-    sp_count = lax.axis_size(SP)
-    tp_count = lax.axis_size("tp")
-    exp_dev = gate_up_weight.shape[0]
-    experts = exp_dev * sp_count
-    capacity = 3 * TOPK * tok_rows // (2 * tp_count * experts)
-    model_width = normed.shape[1]
-    flat_experts = selected_experts.reshape(-1)
-    member = (flat_experts[:, None] == jnp.arange(experts, dtype=jnp.int32)[None, :]).astype(
-        jnp.int32
-    )
-    slot_rank = jnp.sum(jnp.cumsum(member, axis=0) * member, axis=1) - 1
-    slot_index = flat_experts * capacity + slot_rank
-    slot_hot = (
-        slot_index[:, None] == jnp.arange(experts * capacity, dtype=jnp.int32)[None, :]
-    ).astype(jnp.bfloat16)
-    token_hot = jnp.sum(slot_hot.reshape(local_rows, TOPK, experts * capacity), axis=1)
-    outgoing = jnp.einsum(
-        "rs,rd->sd", token_hot, normed, preferred_element_type=jnp.float32
-    ).astype(jnp.bfloat16)
-    grouped = outgoing.reshape(sp_count, exp_dev, capacity, model_width)
-    copies = jnp.broadcast_to(
-        grouped[:, None], (sp_count, tp_count, exp_dev, capacity, model_width)
-    )
-    copies = copies.reshape(sp_count * tp_count, exp_dev, capacity, model_width)
-    arrived = lax.all_to_all(copies, SP_TP, split_axis=0, concat_axis=0, tiled=True)
-    gate_pre = jnp.einsum(
-        "secd,edf->secf", arrived, gate_up_weight, preferred_element_type=jnp.float32
-    )
-    linear_pre = jnp.einsum(
-        "secd,edf->secf", arrived, linear_up_weight, preferred_element_type=jnp.float32
-    )
-    clipped = jnp.minimum(gate_pre, 7.0)
-    hidden_act = (
-        clipped * jax.nn.sigmoid(1.702 * clipped) * (jnp.clip(linear_pre, -7.0, 7.0) + 1.0)
-    ).astype(jnp.bfloat16)
-    partial_value = jnp.einsum(
-        "secf,efd->secd", hidden_act, down_weight, preferred_element_type=jnp.float32
-    )
-    summed = lax.psum_scatter(
-        partial_value.reshape(sp_count, tp_count, exp_dev, capacity, model_width).astype(
-            jnp.bfloat16
-        ),
-        "tp",
-        scatter_dimension=1,
-        tiled=True,
-    )
-    returned = lax.all_to_all(summed, SP, split_axis=0, concat_axis=0, tiled=True)
-    returned = returned.reshape(experts * capacity, model_width)
-    picked = jnp.dot(slot_hot, returned, preferred_element_type=jnp.float32).reshape(
-        local_rows, TOPK, model_width
-    )
-    combined = jnp.sum(picked * route_weight[:, :, None], axis=1)
-    return (stream_wide + combined).astype(jnp.bfloat16)
+    return expert_layer(
+        stream[: residual.shape[0]],
+        normed,
+        selected_experts,
+        selected_2,
+        route_weight,
+        gate_up_weight[0],
+        linear_up_weight[0],
+        down_quarter,
+    )
 
 
 def solution(mesh):

time: 629 us -> 337 us (0.54); the launches traced: 620 us -> 336 us
  Pallas kernels: 51.5 us -> 271 us
  waiting for transfers between devices: 210 us -> 7.55 us
  blocking collectives: 196 us -> 0 us
  local copies, waits for them, and re-layouts: 74.8 us -> 17.5 us
  matrix products: 52.9 us -> 16 us
  starting transfers between devices: 12.5 us -> 3.69 us
    pallas_call x0 -> x2, Pallas kernels: none -> 203 us  [the longest x1 175 us: dispatch(): pl.pallas_call(dispatch_kernel, in_specs=[vmem, far_off, far_off, far_off...]
    all_to_all x1 -> x0, blocking collectives: 196 us -> none  [per_device(): lax.all_to_all(copies, SP_TP, split_axis=0, concat_axis=0, tiled=True)]
    reduce_scatter x1 -> x0, waiting for transfers between devices: 110 us -> none  [per_device(): lax.psum_scatter(partial_value.reshape(sp_count, tp_count, exp_dev, capac...]
    all_to_all x2 -> x0, waiting for transfers between devices: 100 us -> none  [the longest x1 53.9 us: per_device(): lax.all_to_all(summed, SP, split_axis=0, concat_axis=0, tiled=True)]
    dot_general x5 -> x2, matrix products: 52.9 us -> 16 us  [the longest x1 11.3 us: per_device(): mix_sum = jnp.dot(head_mix, full_weight, preferred_element_type=jnp.float32)]
    convert_element_type x2 -> x0, local copies, waits for them, and re-layouts: 33.7 us -> none  [per_device(): partial_value.reshape(sp_count, tp_count, exp_dev, capacity, model_width)]
    pallas_call x1, Pallas kernels: 36.1 us -> 52.7 us  [exchange(): pl.pallas_call(exchange_kernel, in_specs=[pl.BlockSpec(memory_space=pltpu...]
    all_to_all x2 -> x0, starting transfers between devices: 12.5 us -> none  [the longest x1 7.53 us: per_device(): lax.all_to_all(summed, SP, split_axis=0, concat_axis=0, tiled=True)]
  transfers between devices with their start and end apart: 3 -> 3, of which waited for: 3 -> 1; matrix products, arithmetic and copies ran while one was open for 0% -> 3% of each run, Pallas kernels for 0% -> 29%
where the time goes in v3:
time: 337 us; the launch traced here: 336 us
  Pallas kernels  271 us (80%)
  local copies, waits for them, and re-layouts  17.5 us (5%)
  matrix products  16 us (5%)
  between operations  13.6 us (4%)
  waiting for transfers between devices  7.55 us (2%)
  other arithmetic  6.64 us (2%)
  starting transfers between devices  3.69 us (1%)
    pallas_call x1, Pallas kernels, dispatch(): pl.pallas_call(dispatch_kernel, in_specs=[vmem, far_off, far_off, far_off...  175 us
    pallas_call x1, Pallas kernels, exchange(): pl.pallas_call(exchange_kernel, in_specs=[pl.BlockSpec(memory_space=pltpu...  52.7 us
    pallas_call x1, Pallas kernels, swap(): pl.pallas_call(swap_kernel, in_specs=[pl.BlockSpec(memory_space=pltpu.VME...  27.9 us
    pallas_call x1, Pallas kernels, local_pass(): pl.pallas_call(local_kernel, grid=(heads,), in_specs=[columns, columns, c...  12.1 us
    unnamed x26, local copies, waits for them, and re-layouts  12 us
    dot_general x1, matrix products, per_device(): mix_sum = jnp.dot(head_mix, full_weight, preferred_element_type=jnp.float32)  11.3 us
    all_gather x1, waiting for transfers between devices, per_device(): full_weight = lax.all_gather(own_rows, ('tp',) + SP, axis=0, tiled=True)  7.52 us
  transfers between devices with their start and end apart: 3, of which 1 were waited for; matrix products, arithmetic and copies ran while one was open for 3% of the time, Pallas kernels for 29%

profile of v3, /device:TPU:0, one launch (start us, length us, event | category | flops | bytes accessed | tf_op | source)
XLA Modules:
  0.0 336.4 jit_solution(2145319478186888534)
XLA Ops:
  6.5 0.0 all-gather.2.cloned.1.call-start
  6.5 1.6 constant_dynamic-slice_fusion
  8.1 0.0 all-gather.2.cloned.1.call-update
  8.1 3.2 collective-permute-start.1
  11.3 0.8 copy.99
  12.1 0.5 collective-permute-start
  12.6 0.1 eq.371
  12.7 0.1 eq.375
  12.9 0.7 neg.11
  13.6 0.8 fusion.50
  14.4 0.7 divide_bitcast_fusion
  15.2 0.6 reduce-window.14
  15.8 0.2 slice_reduce_fusion.1
  16.0 0.1 fusion.45
  16.1 0.1 sub.80
  16.3 0.7 broadcast_compare_fusion
  17.0 0.1 copy.113
  17.1 0.1 copy.110
  17.2 0.1 copy.104
  17.4 0.4 fusion.37
  17.8 0.1 copy.124
  17.8 0.1 copy.123
  17.9 0.7 exponential_reduce_fusion
  18.6 0.1 copy.125
  18.8 0.7 broadcast_divide_fusion.weight_ref
  19.5 0.0 copy-start.7
  19.5 1.0 copy-done.7
  20.5 0.0 copy-start.8
  20.5 1.0 copy-done.8
  21.6 1.0 copy-done.9
  22.6 12.1 %local_pass.1 = (f32[512,512]{1,0:T(8,128)S(1)}, bf16[4,512,256]{2,1,0:T(8,128)(2,1)S(1)}, bf16[4,8,128,256]{3,2,1,0:T(8,128)(2,1)}, bf16[4,2,128,256]{3,2,1,0:T(8,128)(2,1)S(1)}) custom-call(bf16[512,512]{1,0:T(8,128)(2,1)S(1)} %copy-done.7, bf16[512,512]{1,0:T(8,128)(2,1)S(1)} %copy-done.8, bf16[512,512]{1,0:T(8,128)(2,1)S(1)} %copy-done.9, ...), custom_call_target="tpu_custom_call" | custom-call | flops 4000000000 | bytes 8000000 | tf_op jit(solution)/shard_map/local_pass/pallas_call | solution.py:118
  34.7 1.0 copy-done.2
  35.7 0.8 copy-done.10
  36.5 52.7 %exchange.1 = (bf16[8,128,128]{2,1,0:T(8,128)(2,1)}, bf16[1536,1024]{1,0:T(8,128)(2,1)}) custom-call(bf16[8,128,256]{2,1,0:T(8,128)(2,1)} %bitcast.56, bf16[384,4096]{1,0:T(8,128)(2,1)} %bitcast.64), custom_call_target="tpu_custom_call" | custom-call | flops 8999999488 | bytes 8000000 | tf_op jit(solution)/shard_map/exchange/pallas_call | solution.py:330
  89.2 0.0 copy-start.11
  89.2 0.0 copy-done
  89.2 0.0 copy-done.6
  89.2 0.0 copy-start.3
  89.3 1.2 copy-done.3
  90.5 1.0 copy-done.4
  91.5 0.9 copy-done.5
  92.5 3.3 finish_pass.1.mix_ref
  95.8 0.0 copy-start.1
  95.8 0.8 copy-done.1
  96.6 27.9 %swap.1 = bf16[256,2048]{1,0:T(8,128)(2,1)} custom-call(bf16[512,512]{1,0:T(8,128)(2,1)} %copy-done.1), custom_call_target="tpu_custom_call" | custom-call | tf_op jit(solution)/shard_map/swap/pallas_call | solution.py:446
  124.5 0.0 copy-done.11
  124.5 0.1 copy.119
  124.6 0.9 copy.126.index_ref
  125.5 0.0 collective-permute-done
  125.5 0.1 eq.414
  125.6 0.6 reduce-window.16
  126.2 0.2 slice_reduce_fusion
  126.4 0.1 eq.410
  126.6 0.1 fusion.43
  126.7 0.1 sub.88
  126.8 0.4 add_add_fusion
  127.2 0.1 copy.120
  127.3 0.0 collective-permute-done.1
  127.3 7.5 %all-gather.2.cloned.1.call-done = bf16[2048,4096]{1,0:T(8,128)(2,1)} async-done(((bf16[16,4096]{1,0:T(8,128)(2,1)}), bf16[2048,4096]{1,0:T(8,128)(2,1)}) %all-gather.2.cloned.1.call-update) | async-done | bytes 16777232 | tf_op jit(solution)/shard_map/all_gather | solution.py:797
  134.8 11.3 %fusion = (f32[256]{0:T(256)S(1)}, bf16[256,4096]{1,0:T(8,128)(2,1)S(1)}) fusion(bf16[128,4096]{1,0:T(8,128)(2,1)} %collective-permute-done.1, bf16[128,4096]{1,0:T(8,128)(2,1)} %param.27, bf16[256,2048]{1,0:T(8,128)(2,1)} %swap.1, bf16[2048,4096]{1,0:T(8,128)(2,1)} %all-gather.2.cloned.1.call-done), kind=kOutput, calls=%fused_computation.3 | convolution fusion | flops 4304404480 | bytes 22021120 | tf_op jit(solution)/shard_map/dot_general | solution.py:813
  146.2 1.1 slice.32.stream_ref
  147.3 4.7 %convolution_convert_fusion = bf16[768,4096]{1,0:T(8,128)(2,1)} fusion(bf16[256,4096]{1,0:T(8,128)(2,1)S(1)} %get-tuple-element.22, f32[4096]{0:T(1024)S(1)} %convert_element_type.41, f32[256]{0:T(256)S(1)} %add_rsqrt_fusion, s32[256]{0:T(256)S(1)} %bitcast.62, s32[256]{0:T(256)S(1)} %bitcast.61), kind=kOutput, calls=%fused_computation | convolution fusion | flops 1619525632 | bytes 8408064 | tf_op jit(solution)/shard_map/dot_general | solution.py:763
  151.9 175.3 %experts.1 = bf16[128,4096]{1,0:T(8,128)(2,1)} custom-call(bf16[32,24,4096]{2,1,0:T(8,128)(2,1)} %bitcast.57, bf16[4096,384]{1,0:T(8,128)(2,1)} %bitcast.58, bf16[4096,384]{1,0:T(8,128)(2,1)} %bitcast.59, bf16[1536,1024]{1,0:T(8,128)(2,1)} %get-tuple-element.16.down_ref, s32[512,1]{1,0:T(8,128)} %copy.126.index_ref, ...), custom_call_target="tpu_custom_call" | custom-call | tf_op jit(solution)/shard_map/experts/pallas_call | solution.py:712
  327.2 2.3 copy.143
  (24 shorter events, 0.2 us)
Async XLA Ops:
  6.5 128.3 %all-gather.2.cloned.1.call-start = ((), (), s32[]{:S(2)}) async-start(), calls=%async_computation | async-start | bytes 16908288 | tf_op jit(solution)/shard_map/all_gather | solution.py:797
  8.1 119.2 %collective-permute-start.1 = (bf16[128,4096]{1,0:T(8,128)(2,1)}, bf16[128,4096]{1,0:T(8,128)(2,1)}, u32[]{:S(2)}, u32[]{:S(2)}) collective-permute-start(bf16[128,4096]{1,0:T(8,128)(2,1)} %param.27), channel_id=1, source_target_pairs={{0,2},{1,3},{2,0},{3,1},{4,6},{5,7},{6,4},{7,5},{8,10},{9,11},{10,... | collective-permute-start | bytes 3145736 | tf_op jit(solution)/shard_map/ppermute | solution.py:799
  12.1 113.3 %collective-permute-start = (s32[128,2]{1,0:T(8,128)S(1)}, s32[128,2]{1,0:T(8,128)S(1)}, u32[]{:S(2)}, u32[]{:S(2)}) collective-permute-start(s32[128,2]{1,0:T(8,128)S(1)} %copy.99), channel_id=1, source_target_pairs={{0,2},{1,3},{2,0},{3,1},{4,6},{5,7},{6,4},{7,5},{8,10},{9,11},{10,... | collective-permute-start | bytes 3080 | tf_op jit(solution)/shard_map/ppermute | solution.py:800
  19.5 1.0 copy-start.7
  20.5 1.0 copy-start.8
  21.6 1.0 copy-start.9
  34.7 1.0 copy-start.2
  35.7 0.8 copy-start.10
  36.5 52.8 %copy-start = (bf16[4,8,128,256]{3,2,1,0:T(8,128)(2,1)S(1)}, bf16[4,8,128,256]{3,2,1,0:T(8,128)(2,1)}, u32[]{:S(2)}) copy-start(bf16[4,8,128,256]{3,2,1,0:T(8,128)(2,1)} %get-tuple-element.13.blk_ref) | copy-start | bytes 6291460
  36.5 52.8 %copy-start.6 = (bf16[128]{0:T(256)(128)(2,1)S(1)}, bf16[128]{0:T(256)(128)(2,1)}, u32[]{:S(2)}) copy-start(bf16[128]{0:T(256)(128)(2,1)} %param.25) | copy-start | bytes 772
  89.2 35.3 %copy-start.11 = (bf16[4096]{0:T(1024)(128)(2,1)S(1)}, bf16[4096]{0:T(1024)(128)(2,1)}, u32[]{:S(2)}) copy-start(bf16[4096]{0:T(1024)(128)(2,1)} %param.28) | copy-start | bytes 24580
  89.2 1.2 copy-start.3
  90.5 1.0 copy-start.4
  91.5 0.9 copy-start.5
  95.8 0.8 copy-start.1
Sparse Core Ops, SparseCore 0:
  10.5 124.3 all-gather.1
